TPU v7x, 1024 devices: a whole 4x8x16 slice. The times are simulated.
1024 devices in a mesh: sp: 256 (over z, y, core), tp: 4 (over x).
Axes of the slice: x: 4, y: 8, z: 16, core: 2. Of those that a mesh axis runs over, the one named last changes fastest.
Arguments:
- query_rows: bfloat16 [163840, 1536], P('sp', 'tp'), may hold values from -8 to 8
- key_rows: bfloat16 [163840, 1536], P('sp', 'tp'), may hold values from -8 to 8
- value_rows: bfloat16 [163840, 1536], P('sp', 'tp'), may hold values from -6 to 6
- query_gain: bfloat16 [64], replicated, may hold values from 0.25 to 4.2
- key_gain: bfloat16 [64], replicated, may hold values from 0.25 to 4.2
- position_bias: bfloat16 [24, 320], P('tp'), may hold values from -165 to 3
- output_grad: bfloat16 [163840, 1536], P('sp', 'tp'), may hold values from -24 to 24
Outputs:
- query_grad: bfloat16 [163840, 1536], P('sp', 'tp')
- key_grad: bfloat16 [163840, 1536], P('sp', 'tp')
- value_grad: bfloat16 [163840, 1536], P('sp', 'tp')
- bias_grad: float32 [24, 320], P('tp')
- query_gain_grad: float32 [64], replicated
- key_gain_grad: float32 [64], replicated
All inputs are finite; a program needn't handle non-finite values.
Results may differ from a plain program's by a relative error of at most 0.0055.
The roundings to bfloat16 on the way count: a program that leaves them out, or rounds other values in their place, can miss the bound.
Values may be sent and summed in bfloat16 or wider, within the bound.
No kernel may reach another device: no remote copies, remote signals or barrier semaphores. Data moves between devices by JAX's collectives and lax.ppermute only.
A program may use at most 128 MiB of HBM per device.

v0:
```python
import functools

import jax
import jax.numpy as jnp
import numpy as np
from jax import lax
from jax.sharding import Mesh
from jax.sharding import PartitionSpec as P

SEG = 64
LEFT = 8
BAND = 576
RSPAN = 320
SP = ("sp_0", "sp_1", "sp_2")
SP_TP = ("sp_0", "sp_1", "sp_2", "tp")


NORM_EPS = 1e-06


def passed_along(block, axis, distance):
    devices = range(lax.axis_size(axis))
    route = [(i - distance, i) for i in devices if i - distance in devices]
    return lax.ppermute(block, axis, route)


def by_axis(value, axes):
    return functools.reduce(lax.psum, axes, value)


def unit_rows(values):
    widened = values.astype(jnp.float32)
    scale_rows = lax.rsqrt(jnp.mean(widened * widened, axis=-1, keepdims=True) + NORM_EPS)
    return (widened * scale_rows, scale_rows)


def band_of(segments, seg_count):
    return jnp.concatenate(
        [segments[offset : offset + seg_count] for offset in range(LEFT + 1)], axis=1
    )


def unband(banded, seg_count):
    summed = jnp.zeros((seg_count + LEFT, SEG) + banded.shape[2:], jnp.float32)
    for offset in range(LEFT + 1):
        summed = summed.at[offset : offset + seg_count].add(
            banded[:, offset * SEG : (offset + 1) * SEG]
        )
    return summed


def head_major(matrix, head_count):
    return matrix.reshape(matrix.shape[0], head_count, -1).transpose(1, 0, 2)


def row_major(stacked):
    return stacked.transpose(1, 0, 2).reshape(stacked.shape[1], -1)


def bias_matrix_of(bias_table):
    head_count = bias_table.shape[0]
    extent = BAND + SEG - 1
    tail_fill = jnp.broadcast_to(bias_table[:, -1:], (head_count, extent - bias_table.shape[1]))
    extended = jnp.concatenate([bias_table, tail_fill], axis=1)
    shifted = jnp.roll(extended[:, ::-1], -(SEG - 1), axis=1)
    tiled = jnp.tile(shifted, (1, SEG))[:, : SEG * (extent - 1)]
    return tiled.reshape(head_count, SEG, extent - 1)[:, :, :BAND]


def bias_grad_of(summed):
    head_count = summed.shape[0]
    extent = BAND + SEG - 1
    padded = jnp.pad(summed[:, ::-1, :], ((0, 0), (0, 0), (0, SEG)))
    skewed = padded.reshape(head_count, SEG * (extent + 1))[:, : SEG * extent].reshape(
        head_count, SEG, extent
    )
    by_distance = jnp.sum(skewed, axis=1)[:, ::-1]
    return jnp.concatenate(
        [by_distance[:, : RSPAN - 1], jnp.sum(by_distance[:, RSPAN - 1 :], axis=1, keepdims=True)],
        axis=1,
    )


def backward_block(query_seg, grad_seg, key_band, value_band, row_bias, visible):
    score_scale = query_seg.shape[-1] ** (-0.5)
    scores = (
        jnp.einsum("cqd,ckd->cqk", query_seg, key_band, preferred_element_type=jnp.float32)
        * score_scale
        + row_bias[None]
    )
    scores = jnp.where(visible[:, None, :], scores, -jnp.inf)
    d_weights = jnp.einsum("cqd,ckd->cqk", grad_seg, value_band, preferred_element_type=jnp.float32)
    row_peak = jnp.max(scores, axis=-1)
    raised = jnp.exp(scores - row_peak[..., None])
    row_total = jnp.sum(raised, axis=-1)
    weights = raised / row_total[..., None]
    row_delta = jnp.sum(weights * d_weights, axis=-1)
    d_scores = weights * (d_weights - row_delta[..., None])
    weights_low = weights.astype(jnp.bfloat16)
    d_low = d_scores.astype(jnp.bfloat16)
    dq_unit = (
        jnp.einsum("cqk,ckd->cqd", d_low, key_band, preferred_element_type=jnp.float32)
        * score_scale
    )
    dk_band = (
        jnp.einsum("cqk,cqd->ckd", d_low, query_seg, preferred_element_type=jnp.float32)
        * score_scale
    )
    dv_band = jnp.einsum("cqk,cqd->ckd", weights_low, grad_seg, preferred_element_type=jnp.float32)
    return (dq_unit, dk_band, dv_band, d_scores, (row_peak, row_total, row_delta))


def body(query_rows, key_rows, value_rows, query_gain, key_gain, position_bias, output_grad):
    head_count = position_bias.shape[0]
    tokens = query_rows.shape[0]
    head_size = query_gain.shape[0]
    seg_count = tokens // SEG
    reach_rows = LEFT * SEG
    gain_query = query_gain.astype(jnp.float32)
    gain_key = key_gain.astype(jnp.float32)
    query_hat, query_scale = unit_rows(head_major(query_rows, head_count))
    key_hat, key_scale = unit_rows(head_major(key_rows, head_count))
    query_unit = (query_hat * gain_query).astype(jnp.bfloat16)
    key_unit = (key_hat * gain_key).astype(jnp.bfloat16)
    value_heads = head_major(value_rows, head_count)
    cotangent_heads = head_major(output_grad, head_count)
    bias_mats = bias_matrix_of(position_bias.astype(jnp.float32))
    band_pos = np.repeat(np.arange(LEFT + 1), SEG)
    first_seg = lax.axis_index(SP) * seg_count
    visible = first_seg + jnp.arange(seg_count)[:, None] - LEFT + band_pos[None, :] >= 0
    prior_key, prior_value = passed_along(
        (
            key_unit[:, tokens - reach_rows :].reshape(head_count, reach_rows * head_size),
            value_heads[:, tokens - reach_rows :].reshape(head_count, reach_rows * head_size),
        ),
        SP,
        1,
    )
    key_ext = jnp.concatenate(
        [prior_key.reshape(head_count, reach_rows, head_size), key_unit], axis=1
    )
    key_ext = key_ext.reshape(head_count, seg_count + LEFT, SEG, head_size)
    value_ext = jnp.concatenate(
        [prior_value.reshape(head_count, reach_rows, head_size), value_heads], axis=1
    )
    value_ext = value_ext.reshape(head_count, seg_count + LEFT, SEG, head_size)

    def main_head(inputs):
        query_head, grad_head, key_segs, value_segs, row_bias = inputs
        outputs = backward_block(
            query_head.reshape(seg_count, SEG, head_size),
            grad_head.reshape(seg_count, SEG, head_size),
            band_of(key_segs, seg_count),
            band_of(value_segs, seg_count),
            row_bias,
            visible,
        )
        return (
            outputs[0].reshape(tokens, head_size),
            unband(outputs[1], seg_count),
            unband(outputs[2], seg_count),
            jnp.sum(outputs[3], axis=0),
            outputs[4],
        )

    dq_unit, dk_ext, dv_ext, score_sums, row_stats = lax.map(
        main_head, (query_unit, cotangent_heads, key_ext, value_ext, bias_mats)
    )
    dk_unit = dk_ext[:, LEFT:].reshape(head_count, tokens, head_size)
    dv_own = dv_ext[:, LEFT:].reshape(head_count, tokens, head_size)
    back_key, back_value = passed_along(
        (
            dk_ext[:, :LEFT].reshape(head_count, reach_rows * head_size).astype(jnp.bfloat16),
            dv_ext[:, :LEFT].reshape(head_count, reach_rows * head_size).astype(jnp.bfloat16),
        ),
        SP,
        -1,
    )
    from_later_key = back_key.reshape(head_count, reach_rows, head_size).astype(jnp.float32)
    from_later_value = back_value.reshape(head_count, reach_rows, head_size).astype(jnp.float32)
    front_pad = ((0, 0), (tokens - reach_rows, 0), (0, 0))
    dk_unit = dk_unit + jnp.pad(from_later_key, front_pad)
    value_grad = dv_own + jnp.pad(from_later_value, front_pad)
    bias_part = bias_grad_of(score_sums)
    query_gain_part = jnp.sum(dq_unit * query_hat, axis=(0, 1))
    key_gain_part = jnp.sum(dk_unit * key_hat, axis=(0, 1))
    zero_index = jnp.zeros((), jnp.int32)
    head_start = lax.axis_index("tp") * head_count
    full_table = jnp.zeros((head_count * lax.axis_size("tp"), bias_part.shape[1]), jnp.float32)
    full_table = lax.dynamic_update_slice(full_table, bias_part, (head_start, zero_index))
    full_table, query_gain_grad, key_gain_grad = (
        by_axis(full_table, SP_TP),
        by_axis(query_gain_part, SP_TP),
        by_axis(key_gain_part, SP_TP),
    )
    bias_grad = lax.dynamic_slice(
        full_table, (head_start, zero_index), (head_count, bias_part.shape[1])
    )
    dq_scaled = dq_unit * gain_query
    query_grad = query_scale * (
        dq_scaled - query_hat * jnp.mean(dq_scaled * query_hat, axis=-1, keepdims=True)
    )
    dk_scaled = dk_unit * gain_key
    key_grad = key_scale * (
        dk_scaled - key_hat * jnp.mean(dk_scaled * key_hat, axis=-1, keepdims=True)
    )
    return (
        row_major(query_grad.astype(jnp.bfloat16)),
        row_major(key_grad.astype(jnp.bfloat16)),
        row_major(value_grad.astype(jnp.bfloat16)),
        bias_grad,
        query_gain_grad,
        key_gain_grad,
    )


def solution(mesh):
    torus = Mesh(mesh.devices.reshape(16, 8, 2, mesh.shape["tp"]), ("sp_0", "sp_1", "sp_2", "tp"))
    placed = (P(SP, "tp"), P(SP, "tp"), P(SP, "tp"), P(), P(), P("tp", None), P(SP, "tp"))
    return jax.shard_map(
        body,
        mesh=torus,
        in_specs=placed,
        out_specs=(P(SP, "tp"), P(SP, "tp"), P(SP, "tp"), P("tp", None), P(), P()),
        check_vma=False,
    )
```

profile of v0, /device:TPU:24, one launch (start us, length us, event | category | flops | bytes accessed | tf_op | source)
XLA Modules:
  0.0 352.5 jit_solution(170472726108736063)
XLA Ops:
  5.6 1.9 collective-permute-start
  9.7 4.8 %collective-permute-start.1 = (bf16[6,32768]{1,0:T(8,128)(2,1)}, bf16[6,32768]{1,0:T(8,128)(2,1)}, u32[]{:S(2)}, u32[]{:S(2)}) collective-permute-start(bf16[6,32768]{1,0:T(8,128)(2,1)} %reshape.769), channel_id=1, source_target_pairs={{0,4},{4,8},{8,12},{12,16},{16,20},{20,24},{24,28},{28,32},{32,36}... | collective-permute-start | bytes 1179656 | tf_op jit(solution)/shard_map/ppermute | solution.py:24
  18.0 2.0 reshape.766
  21.0 1.8 reshape.764
  23.2 2.8 reshape.765
  26.0 2.1 copy.31
  28.1 1.8 reshape.770
  30.3 2.9 reshape.771
  33.2 3.4 copy.33
  36.6 148.7 %while.38 = (s32[]{:T(128)}, f32[6,640,64]{1,2,0:T(8,128)}, f32[6,18,64,64]{2,3,1,0:T(8,128)}, f32[6,18,64,64]{2,3,1,0:T(8,128)}, f32[6,64,576]{2,1,0:T(8,128)},...) while((s32[]{:T(128)}, f32[6,640,64]{1,2,0:T(8,128)}, ...), condition=%wide.region_7.8_spmd.clone, body=%wide.region_2.7_spmd.clone.sunk | while | flops 242498752 | bytes 51985400 | solution.py:166
  36.6 3.1 dynamic-slice_bitcast_fusion.21
  39.7 3.4 concatenate.91
  45.3 1.8 exponential_reduce_fusion.2
  47.3 1.9 fusion.112
  51.3 2.7 concatenate.92
  54.0 2.2 multiply_reduce_fusion.2
  61.5 3.0 dynamic-slice_bitcast_fusion.21
  64.5 3.4 concatenate.91
  70.1 1.8 exponential_reduce_fusion.2
  72.0 1.9 fusion.112
  76.0 2.7 concatenate.92
  78.7 2.2 multiply_reduce_fusion.2
  86.2 3.0 dynamic-slice_bitcast_fusion.21
  89.2 3.4 concatenate.91
  94.8 1.8 exponential_reduce_fusion.2
  96.8 1.9 fusion.112
  100.7 2.7 concatenate.92
  103.5 2.2 multiply_reduce_fusion.2
  110.9 3.0 dynamic-slice_bitcast_fusion.21
  114.0 3.4 concatenate.91
  119.6 1.8 exponential_reduce_fusion.2
  121.6 1.9 fusion.112
  125.6 2.7 concatenate.92
  128.3 2.2 multiply_reduce_fusion.2
  135.8 3.0 dynamic-slice_bitcast_fusion.21
  138.8 3.4 concatenate.91
  144.4 1.8 exponential_reduce_fusion.2
  146.3 1.9 fusion.112
  150.3 2.7 concatenate.92
  153.1 2.2 multiply_reduce_fusion.2
  160.5 3.0 dynamic-slice_bitcast_fusion.21
  163.5 3.4 concatenate.91
  169.1 1.8 exponential_reduce_fusion.2
  171.1 1.9 fusion.112
  175.0 2.7 concatenate.92
  177.8 2.2 multiply_reduce_fusion.2
  188.7 1.9 collective-permute-start.2
  190.6 1.7 slice.848
  192.3 2.9 rev.2
  195.8 2.0 reshape.778
  199.2 3.1 slice.850
  202.3 1.5 slice.1043
  203.9 1.9 copy.35
  205.7 2.1 copy.38
  208.7 2.8 copy.39
  212.7 2.7 convert_element_type.92
  215.4 1.9 collective-permute-start.3
  217.6 2.7 convert_element_type.90
  223.5 2.0 copy.45
  226.8 68.9 %all-reduce.5 = (f32[24,320]{1,0:T(8,128)S(1)}, f32[64]{0:T(128)S(1)}, f32[64]{0:T(128)S(1)}) all-reduce(f32[24,320]{1,0:T(8,128)S(1)} %dynamic_update_slice.34, f32[64]{0:T(128)S(1)} %get-tuple-element.549, f32[64]{0:T(128)S(1)} %get-tuple-element.473), channel_id=1, replica_groups=mesh['sp_0'=16,'sp_1'=8,'sp_2'=2,'tp'=4] {'sp_0'}, use_global_device_ids=true, to_apply=%region_12.13 | all-reduce | flops 7808 | bytes 62464 | tf_op jit(solution)/shard_map/psum | solution.py:28
  295.7 29.4 %all-reduce.6 = (f32[24,320]{1,0:T(8,128)S(1)}, f32[64]{0:T(128)S(1)}, f32[64]{0:T(128)S(1)}) all-reduce(f32[24,320]{1,0:T(8,128)S(1)} %get-tuple-element.501, f32[64]{0:T(128)S(1)} %get-tuple-element.502, f32[64]{0:T(128)S(1)} %get-tuple-element.503), channel_id=1, replica_groups=mesh['sp_0'=16,'sp_1'=8,'sp_2'=2,'tp'=4] {'sp_1'}, use_global_device_ids=true, to_apply=%region_13.14 | all-reduce | flops 7808 | bytes 62464 | tf_op jit(solution)/shard_map/psum | solution.py:28
  325.0 3.5 all-reduce.8
  328.5 17.8 %all-reduce.7 = (f32[24,320]{1,0:T(8,128)S(1)}, f32[64]{0:T(128)}, f32[64]{0:T(128)}) all-reduce(f32[24,320]{1,0:T(8,128)S(1)} %get-tuple-element.510, f32[64]{0:T(128)S(1)} %get-tuple-element.511, f32[64]{0:T(128)S(1)} %get-tuple-element.512), channel_id=1, replica_groups=mesh['sp_0'=16,'sp_1'=8,'sp_2'=2,'tp'=4] {'tp'}, use_global_device_ids=true, to_apply=%region_15.16 | all-reduce | flops 7808 | bytes 62464 | tf_op jit(solution)/shard_map/psum | solution.py:28
  347.0 2.7 convert_element_type.93
  (372 shorter events, 84.5 us)
Async XLA Ops:
  1.9 2.2 copy-start.3
  2.1 0.8 copy-start.17
  2.9 0.8 copy-start.12
  3.7 3.8 %copy-start.14 = (bf16[640,384]{1,0:T(8,128)(2,1)S(1)}, bf16[640,384]{1,0:T(8,128)(2,1)}, u32[]{:S(2)}) copy-start(bf16[640,384]{1,0:T(8,128)(2,1)} %param.48) | copy-start | bytes 1474564
  5.6 15.4 %collective-permute-start = (bf16[6,32768]{1,0:T(8,128)(2,1)}, bf16[6,32768]{1,0:T(8,128)(2,1)}, u32[]{:S(2)}, u32[]{:S(2)}) collective-permute-start(bf16[6,32768]{1,0:T(8,128)(2,1)} %reshape.763), channel_id=1, source_target_pairs={{0,4},{4,8},{8,12},{12,16},{16,20},{20,24},{24,28},{28,32},{32,36}... | collective-permute-start | bytes 1179656 | tf_op jit(solution)/shard_map/ppermute | solution.py:24
  7.8 1.9 copy-start.10
  7.8 6.7 %copy-start.15 = (bf16[640,384]{1,0:T(8,128)(2,1)S(1)}, bf16[640,384]{1,0:T(8,128)(2,1)}, u32[]{:S(2)}) copy-start(bf16[640,384]{1,0:T(8,128)(2,1)} %param.46) | copy-start | bytes 1474564
  8.2 6.7 %copy-start.24 = (bf16[64]{0:T(256)(128)(2,1)S(1)}, bf16[64]{0:T(256)(128)(2,1)}, u32[]{:S(2)}) copy-start(bf16[64]{0:T(256)(128)(2,1)} %param.49) | copy-start | bytes 388
  8.3 6.7 %copy-start.23 = (bf16[6,320]{1,0:T(8,128)(2,1)S(1)}, bf16[6,320]{1,0:T(8,128)(2,1)}, u32[]{:S(2)}) copy-start(bf16[6,320]{1,0:T(8,128)(2,1)} %param.51) | copy-start | bytes 11524
  9.7 18.4 %collective-permute-start.1 = (bf16[6,32768]{1,0:T(8,128)(2,1)}, bf16[6,32768]{1,0:T(8,128)(2,1)}, u32[]{:S(2)}, u32[]{:S(2)}) collective-permute-start(bf16[6,32768]{1,0:T(8,128)(2,1)} %reshape.769), channel_id=1, source_target_pairs={{0,4},{4,8},{8,12},{12,16},{16,20},{20,24},{24,28},{28,32},{32,36}... | collective-permute-start | bytes 1179656 | tf_op jit(solution)/shard_map/ppermute | solution.py:24
  14.8 3.1 copy-start.5
  15.0 2.1 copy-start.19
  18.0 2.0 copy-start.16
  20.0 3.1 copy-start.13
  28.1 2.1 copy-start.11
  33.2 3.4 copy-start.21
  44.2 2.9 copy-start.1
  47.3 2.0 copy-start.8
  54.0 2.2 copy-start
  56.2 0.9 copy-start.2
  69.0 2.9 copy-start.1
  72.0 2.0 copy-start.8
  78.7 2.2 copy-start
  80.9 0.9 copy-start.2
  93.7 2.9 copy-start.1
  96.8 2.0 copy-start.8
  103.5 2.2 copy-start
  105.7 0.9 copy-start.2
  118.5 2.9 copy-start.1
  121.6 2.0 copy-start.8
  128.3 2.2 copy-start
  130.5 0.9 copy-start.2
  143.3 2.9 copy-start.1
  146.3 2.0 copy-start.8
  153.0 2.2 copy-start
  155.2 0.9 copy-start.2
  168.0 2.9 copy-start.1
  171.1 2.0 copy-start.8
  177.8 2.2 copy-start
  180.0 0.9 copy-start.2
  188.7 28.9 %collective-permute-start.2 = (bf16[6,32768]{1,0:T(8,128)(2,1)}, bf16[6,32768]{1,0:T(8,128)(2,1)}, u32[]{:S(2)}, u32[]{:S(2)}) collective-permute-start(bf16[6,32768]{1,0:T(8,128)(2,1)} %convert_element_type.89), channel_id=1, source_target_pairs={{4,0},{8,4},{12,8},{16,12},{20,16},{24,20},{28,24},{32,28},{36,32}... | collective-permute-start | bytes 1179656 | tf_op jit(solution)/shard_map/ppermute | solution.py:24
  199.1 3.2 copy-start.22
  205.7 2.4 slice-start
  212.7 9.0 %copy-start.4 = (bf16[640,384]{0,1:T(8,128)(2,1)S(1)}, bf16[640,384]{0,1:T(8,128)(2,1)}, u32[]{:S(2)}) copy-start(bf16[640,384]{0,1:T(8,128)(2,1)} %copy-done.3) | copy-start | bytes 1474564
  212.7 9.0 %copy-start.6 = (bf16[640,384]{0,1:T(8,128)(2,1)S(1)}, bf16[640,384]{0,1:T(8,128)(2,1)}, u32[]{:S(2)}) copy-start(bf16[640,384]{0,1:T(8,128)(2,1)} %copy-done.5) | copy-start | bytes 1474564
  212.7 9.0 %copy-start.9 = (f32[6,640,64]{1,2,0:T(8,128)S(1)}, f32[6,640,64]{1,2,0:T(8,128)}, u32[]{:S(2)}) copy-start(f32[6,640,64]{1,2,0:T(8,128)} %get-tuple-element.423) | copy-start | bytes 2949124
  212.7 9.0 %copy-start.18 = (f32[6,640]{1,0:T(8,128)S(1)}, f32[6,640]{1,0:T(8,128)}, u32[]{:S(2)}) copy-start(f32[6,640]{1,0:T(8,128)} %copy-done.17) | copy-start | bytes 46084
  212.7 9.0 %copy-start.20 = (f32[6,640]{1,0:T(8,128)S(1)}, f32[6,640]{1,0:T(8,128)}, u32[]{:S(2)}) copy-start(f32[6,640]{1,0:T(8,128)} %copy-done.19) | copy-start | bytes 46084
  215.4 131.5 %collective-permute-start.3 = (bf16[6,32768]{1,0:T(8,128)(2,1)}, bf16[6,32768]{1,0:T(8,128)(2,1)}, u32[]{:S(2)}, u32[]{:S(2)}) collective-permute-start(bf16[6,32768]{1,0:T(8,128)(2,1)} %convert_element_type.92), channel_id=1, source_target_pairs={{4,0},{8,4},{12,8},{16,12},{20,16},{24,20},{28,24},{32,28},{36,32}... | collective-permute-start | bytes 1179656 | tf_op jit(solution)/shard_map/ppermute | solution.py:24
  225.8 123.9 %copy-start.7 = (f32[6,10,64,64]{3,2,1,0:T(8,128)S(1)}, f32[6,10,64,64]{3,2,1,0:T(8,128)}, u32[]{:S(2)}) copy-start(f32[6,10,64,64]{3,2,1,0:T(8,128)} %copy.39) | copy-start | bytes 2949124
where the time goes:
time: 356 us; the launch traced here: 352 us
  local copies, waits for them, and re-layouts  156 us (44%)
  blocking collectives  120 us (34%)
  matrix products  40.4 us (11%)
  other arithmetic  22.7 us (6%)
  starting transfers between devices  10.5 us (3%)
    psum x4, blocking collectives, by_axis(): return functools.reduce(lax.psum, axes, value)  120 us
    concatenate x12, local copies, waits for them, and re-layouts, band_of(): jnp.concatenate([segments[offset:offset + seg_count] for offset in range(...  36.7 us
    dynamic_update_slice x30, local copies, waits for them, and re-layouts, body(): lax.map(main_head, (query_unit, cotangent_heads, key_ext, value_ext, bias...  19.5 us
    slice x6, local copies, waits for them, and re-layouts, band_of(): segments[offset:offset + seg_count]  18.2 us
    unnamed x58, local copies, waits for them, and re-layouts  14.9 us
    dot_general x6, matrix products, backward_block(): jnp.einsum('cqd,ckd->cqk', grad_seg, value_band, preferred_element_type=j...  12.9 us
    dot_general x6, matrix products, backward_block(): jnp.einsum('cqk,cqd->ckd', weights_low, grad_seg, preferred_element_type=...  11.7 us
    scatter-add x96, other arithmetic, unband(): summed.at[offset:offset + seg_count]  11.4 us
  transfers between devices with their start and end apart: 4, of which 0 were waited for; matrix products, arithmetic and copies ran while one was open for 14% of the time, Pallas kernels for 0%

commit v1 on v0

v1 whole, which is shorter than its diff:
```python
import functools

import jax
import jax.numpy as jnp
from jax import lax
from jax.experimental import pallas as pl
from jax.experimental.pallas import tpu as pltpu
from jax.sharding import Mesh
from jax.sharding import PartitionSpec as P


SEG = 64
LEFT = 8
HEAD = 64
LANES = 128
RSPAN = 320
REACH = LEFT * SEG
NORM_EPS = 1e-06
HIDDEN = -1e30
SP = ("sp_0", "sp_1", "sp_2")
F32 = jnp.float32
BF16 = jnp.bfloat16


def iota(shape, dim):
    return lax.broadcasted_iota(jnp.int32, shape, dim)


def dot(left, right, contract):
    return lax.dot_general(left, right, (contract, ((), ())), preferred_element_type=F32)


def half_means(values):
    same_half = (iota((2 * LANES, LANES), 0) % LANES) // HEAD == iota((2 * LANES, LANES), 1) // HEAD
    weights = jnp.where(same_half, 1.0 / HEAD, 0.0).astype(BF16)
    high = values.astype(BF16)
    low = (values - high.astype(F32)).astype(BF16)
    return dot(jnp.concatenate([high, low], axis=1), weights, ((1,), (0,)))


def normed(rows):
    widened = rows.astype(F32)
    scale = lax.rsqrt(half_means(widened * widened) + NORM_EPS)
    return widened * scale, scale


def by_head(rows):
    first = iota(rows.shape, 1) < HEAD
    zero = jnp.zeros_like(rows)
    return jnp.concatenate([jnp.where(first, rows, zero), jnp.where(first, zero, rows)], axis=0)


def fold(values, combine):
    return combine(values.reshape(-1, 8, values.shape[-1]), axis=0)


def toeplitz(row):
    top = pltpu.roll(jnp.broadcast_to(row, (8, LANES)), 0, 1, stride=1, stride_axis=0)
    return jnp.concatenate([top] + [pltpu.roll(top, 8 * i, 1) for i in range(1, 16)], axis=0)


def diagonal_sums(tile):
    rows = tile.shape[0]
    while rows > 8:
        rows //= 2
        tile = tile[:rows] + pltpu.roll(tile[rows:], LANES - rows, 1)
    for step in (4, 2, 1):
        tile = tile + pltpu.roll(pltpu.roll(tile, LANES - step, 1), 8 - step, 0)
    return tile[:1]


def main_kernel(
    first_ref, query_ref, key_ref, value_ref, grad_ref, prior_key_ref, prior_value_ref,
    query_gain_ref, key_gain_ref, table_ref,
    query_grad_ref, dk_ref, dv_ref, cross_ref, copies_ref,
    q_hat_ref, q_scale_ref, q_two_ref, g_two_ref, k_hat_ref, k_ref, k_t_ref, v_ref,
    bias_ref, s_ref, dp_ref, w_low_ref, d_low_ref, d_sum_ref, small_ref,
):
    tokens = query_ref.shape[0]
    steps = tokens // LANES
    wide = LANES * 5
    pair = pl.program_id(0)
    hidden_prior = first_ref[0]

    query_gain = query_gain_ref[...]
    key_gain = key_gain_ref[...]
    q_hat, q_scale = normed(query_ref[...])
    q_hat_ref[...] = q_hat
    q_scale_ref[...] = q_scale
    q_unit = (q_hat * query_gain).astype(BF16) * jnp.asarray(HEAD**-0.5, BF16)
    for m in range(steps):
        rows = slice(m * LANES, (m + 1) * LANES)
        q_two_ref[2 * m * LANES : 2 * (m + 1) * LANES] = by_head(q_unit[rows])
        g_two_ref[2 * m * LANES : 2 * (m + 1) * LANES] = by_head(grad_ref[rows])
    for part_ref, v_part_ref, start in ((prior_key_ref, prior_value_ref, 0), (key_ref, value_ref, REACH)):
        count = part_ref.shape[0]
        k_hat, _ = normed(part_ref[...])
        k_hat_ref[start : start + count] = k_hat
        k_unit = (k_hat * key_gain).astype(BF16)
        k_ref[start : start + count] = k_unit
        k_t_ref[:, start : start + count] = (k_unit * jnp.asarray(HEAD**-0.5, BF16)).T
        v_ref[start : start + count] = v_part_ref[...]

    square = (LANES, LANES)
    after = iota(square, 1) >= iota(square, 0)
    upper = iota(square, 0) < HEAD
    left = iota(square, 1) < HEAD
    for head in range(2):
        lanes = slice(head * LANES, (head + 1) * LANES)
        table = table_ref[0, head : head + 1]
        far = jnp.broadcast_to(table[:, :1], square)
        near = toeplitz(table[:, :LANES])
        middle = toeplitz(table[:, LANES : 2 * LANES])
        outer = toeplitz(table[:, 2 * LANES :])
        bias_ref[0:LANES, lanes] = jnp.where(upper & ~left, HIDDEN, far)
        bias_ref[LANES : 2 * LANES, lanes] = far
        bias_ref[2 * LANES : 3 * LANES, lanes] = jnp.where(after, far, outer)
        bias_ref[3 * LANES : 4 * LANES, lanes] = jnp.where(after, outer, middle)
        bias_ref[4 * LANES : 5 * LANES, lanes] = jnp.where(
            ~upper & left, HIDDEN, jnp.where(after, middle, near)
        )

    far_sum = jnp.zeros((8, 2 * LANES), F32)
    query_gain_sum = jnp.zeros((8, LANES), F32)
    key_gain_sum = jnp.zeros((8, LANES), F32)
    peaks = {}

    def score_block(m, b):
        if m >= steps:
            return
        at = m * LANES
        cols = slice(2 * at, 2 * (at + LANES))
        band = slice(at + b * LANES, at + (b + 1) * LANES)
        rows = slice(b * LANES, (b + 1) * LANES)
        scores = dot(k_ref[band], q_two_ref[cols], ((1,), (1,))) + bias_ref[rows]
        if m + b < 4:
            scores = scores + hidden_prior
        s_ref[m % 2, rows] = scores
        top = fold(scores, jnp.max)
        peaks[m] = top if b == 0 else jnp.maximum(peaks[m], top)
        dp_ref[m % 2, rows] = dot(v_ref[band], g_two_ref[cols], ((1,), (1,)))

    def query_side(m):
        at = m * LANES
        cols = slice(2 * at, 2 * (at + LANES))
        dq_t = dot(k_t_ref[:, at : at + wide], d_low_ref[at : at + wide, cols], ((1,), (0,)))
        dq = jnp.where(iota(square, 0) < HEAD, dq_t[:, :LANES], dq_t[:, LANES:]).T
        here = slice(at, at + LANES)
        q_hat = q_hat_ref[here]
        scaled = dq * query_gain
        mean = half_means(scaled * q_hat)
        query_grad_ref[here] = (q_scale_ref[here] * (scaled - q_hat * mean)).astype(BF16)
        return fold(dq * q_hat, jnp.sum)

    def key_side(j, low, high):
        band = slice(j * LANES, (j + 1) * LANES)
        cols = slice(2 * low * LANES, 2 * high * LANES)
        dk = dot(d_low_ref[band, cols], q_two_ref[cols], ((1,), (0,)))
        dv = dot(w_low_ref[band, cols], g_two_ref[cols], ((1,), (0,)))
        return dk, dv

    for b in range(5):
        score_block(0, b)
    for m in range(steps):
        at = m * LANES
        cols = slice(2 * at, 2 * (at + LANES))
        peak = jnp.max(peaks[m], axis=0, keepdims=True)
        total = jnp.zeros((8, 2 * LANES), F32)
        delta = jnp.zeros((8, 2 * LANES), F32)
        for b in range(5):
            rows = slice(b * LANES, (b + 1) * LANES)
            raised = jnp.exp(s_ref[m % 2, rows] - peak)
            s_ref[m % 2, rows] = raised
            total = total + fold(raised, jnp.sum)
            delta = delta + fold(raised * dp_ref[m % 2, rows], jnp.sum)
            score_block(m + 1, b)
        inverse = 1.0 / jnp.sum(total, axis=0, keepdims=True)
        delta = jnp.sum(delta, axis=0, keepdims=True) * inverse
        if m > 0:
            query_gain_sum = query_gain_sum + query_side(m - 1)
        for b in range(5):
            rows = slice(b * LANES, (b + 1) * LANES)
            band = slice(at + b * LANES, at + (b + 1) * LANES)
            weights = s_ref[m % 2, rows] * inverse
            d_scores = weights * (dp_ref[m % 2, rows] - delta)
            w_low_ref[band, cols] = weights.astype(BF16)
            d_low_ref[band, cols] = d_scores.astype(BF16)
            if b < 2:
                far_sum = far_sum + fold(d_scores, jnp.sum)
            else:
                kept = slice((b - 2) * LANES, (b - 1) * LANES)
                d_sum_ref[kept] = d_scores if m == 0 else d_sum_ref[kept] + d_scores
        if m < 4:
            dk, dv = key_side(m, 0, m + 1)
            band = slice(m * LANES, (m + 1) * LANES)
            dk_low = dk.astype(BF16)
            cross_ref[band] = dk_low
            cross_ref[REACH + m * LANES : REACH + (m + 1) * LANES] = dv.astype(BF16)
            key_gain_sum = key_gain_sum + fold(dk_low.astype(F32) * k_hat_ref[band], jnp.sum)
        if m == steps - 2:
            for j in range(4, steps + 3):
                dk_ref[(j - 4) * LANES : (j - 3) * LANES], dv_ref[(j - 4) * LANES : (j - 3) * LANES] = key_side(j, j - 4, m + 1)
    query_gain_sum = query_gain_sum + query_side(steps - 1)
    for j in range(4, steps + 4):
        here = slice((j - 4) * LANES, (j - 3) * LANES)
        dk, dv = key_side(j, steps - 1, steps)
        if j < steps + 3:
            dk = dk_ref[here] + dk
            dv = dv_ref[here] + dv
        dk_ref[here] = dk
        dv_ref[here] = dv
        key_gain_sum = key_gain_sum + fold(dk * k_hat_ref[j * LANES : (j + 1) * LANES], jnp.sum)

    tails = []
    for head in range(2):
        lanes = slice(head * LANES, (head + 1) * LANES)
        two, three, four = (d_sum_ref[i * LANES : (i + 1) * LANES, lanes] for i in range(3))
        zero = jnp.zeros(square, F32)
        far = far_sum[:, lanes] + fold(jnp.where(after, two, zero), jnp.sum)
        far = jnp.sum(jnp.sum(far, axis=0, keepdims=True), axis=1, keepdims=True)
        small_ref[pl.ds(5 * pair + 2 * head, 1)] = diagonal_sums(jnp.where(after, four, three))
        small_ref[pl.ds(5 * pair + 2 * head + 1, 1)] = diagonal_sums(jnp.where(after, three, two))
        tail = diagonal_sums(jnp.where(after, zero, four))
        tails.append(jnp.where(iota((1, LANES), 1) == HEAD, far, tail))
    first_half = iota((1, LANES), 1) < HEAD
    small_ref[pl.ds(5 * pair + 4, 1)] = jnp.where(first_half, pltpu.roll(tails[0], HEAD, 1), tails[1])
    both = []
    for part in (query_gain_sum, key_gain_sum):
        part = jnp.sum(part, axis=0, keepdims=True)
        both.append(part + pltpu.roll(part, HEAD, 1))
    gains = jnp.where(first_half, both[0], both[1])

    @pl.when(pair == 0)
    def _():
        small_ref[15:16] = gains

    @pl.when(pair > 0)
    def _():
        small_ref[15:16] = small_ref[15:16] + gains

    @pl.when(pair == pl.num_programs(0) - 1)
    def _():
        for copy in range(copies_ref.shape[0]):
            copies_ref[copy] = small_ref[...]


def final_kernel(key_ref, dk_ref, dv_ref, back_key_ref, back_value_ref, key_gain_ref, key_grad_ref, value_grad_ref):
    tokens = key_ref.shape[0]
    own = tokens - REACH
    for start, count in ((0, own), (own, REACH)):
        rows = slice(start, start + count)
        dk = dk_ref[rows]
        dv = dv_ref[rows]
        if start:
            dk = dk + back_key_ref[...].astype(F32)
            dv = dv + back_value_ref[...].astype(F32)
        value_grad_ref[rows] = dv.astype(BF16)
        k_hat, k_scale = normed(key_ref[rows])
        scaled = dk * key_gain_ref[...]
        mean = half_means(scaled * k_hat)
        key_grad_ref[rows] = (k_scale * (scaled - k_hat * mean)).astype(BF16)


def columns(rows, block=0):
    return pl.BlockSpec((rows, LANES), lambda p: (block, p))


def fixed(shape):
    return pl.BlockSpec(shape, lambda p: (0,) * len(shape))


def main_call(interpret, copies, first, query, key, value, grad, prior, query_gain, key_gain, table):
    tokens, width = query.shape
    pairs = width // LANES
    extended = tokens + REACH
    own = columns(tokens)
    placed = jax.ShapeDtypeStruct if interpret else pltpu.HBM
    return pl.pallas_call(
        main_kernel,
        grid=(pairs,),
        in_specs=[
            pl.BlockSpec(memory_space=pltpu.SMEM), own, own, own, own,
            columns(REACH), columns(REACH, 1), fixed((1, LANES)), fixed((1, LANES)),
            pl.BlockSpec((1, 2, 3 * LANES), lambda p: (p, 0, 0)),
        ],
        out_specs=[own, own, own, columns(2 * REACH), fixed((copies, 16, LANES))],
        out_shape=[
            placed((tokens, width), BF16),
            placed((tokens, width), F32),
            placed((tokens, width), F32),
            placed((2 * REACH, width), BF16),
            placed((copies, 16, LANES), F32),
        ],
        scratch_shapes=[
            pltpu.VMEM((tokens, LANES), F32),
            pltpu.VMEM((tokens, LANES), F32),
            pltpu.VMEM((2 * tokens, LANES), BF16),
            pltpu.VMEM((2 * tokens, LANES), BF16),
            pltpu.VMEM((extended, LANES), F32),
            pltpu.VMEM((extended, LANES), BF16),
            pltpu.VMEM((LANES, extended), BF16),
            pltpu.VMEM((extended, LANES), BF16),
            pltpu.VMEM((5 * LANES, 2 * LANES), F32),
            pltpu.VMEM((2, 5 * LANES, 2 * LANES), F32),
            pltpu.VMEM((2, 5 * LANES, 2 * LANES), F32),
            pltpu.VMEM((extended, 2 * tokens), BF16),
            pltpu.VMEM((extended, 2 * tokens), BF16),
            pltpu.VMEM((3 * LANES, 2 * LANES), F32),
            pltpu.VMEM((16, LANES), F32),
        ],
        compiler_params=None if interpret else pltpu.CompilerParams(vmem_limit_bytes=40 * 2**20),
        interpret=interpret,
        name="band_backward",
    )(first, query, key, value, grad, prior, prior, query_gain, key_gain, table)


def final_call(interpret, key, dk, dv, back, key_gain):
    tokens, width = key.shape
    own = columns(tokens)
    return pl.pallas_call(
        final_kernel,
        grid=(width // LANES,),
        in_specs=[own, own, own, columns(REACH), columns(REACH, 1), fixed((1, LANES))],
        out_specs=[own, own],
        out_shape=[jax.ShapeDtypeStruct((tokens, width), BF16)] * 2,
        interpret=interpret,
        name="key_and_value",
    )(key, dk, dv, back, back, key_gain)


def passed_along(block, axis, distance):
    devices = range(lax.axis_size(axis))
    route = [(i - distance, i) for i in devices if i - distance in devices]
    return lax.ppermute(block, axis, route)


def spread_sum(block, axes):
    return summed_copies(jnp.broadcast_to(block[None], (lax.axis_size(axes),) + block.shape), axes)


def summed_copies(copies, axes):
    return jnp.sum(lax.all_to_all(copies, axes, 0, 0), axis=0)


def body(query_rows, key_rows, value_rows, query_gain, key_gain, position_bias, output_grad, interpret=False):
    tokens = query_rows.shape[0]
    heads = position_bias.shape[0]
    pairs = heads // 2
    sent = jnp.concatenate([key_rows[tokens - REACH :], value_rows[tokens - REACH :]], axis=0)
    prior = passed_along(sent, SP, 1)
    gain_query = jnp.tile(query_gain.astype(F32), 2)[None]
    gain_key = jnp.tile(key_gain.astype(F32), 2)[None]
    table = position_bias.astype(F32)
    table = jnp.concatenate(
        [table[:, -1:], jnp.zeros((heads, 3 * LANES - RSPAN), F32), table[:, :-1]], axis=1
    ).reshape(pairs, 2, 3 * LANES)
    first = jnp.where(lax.axis_index(SP) == 0, HIDDEN, 0.0).astype(F32).reshape(1)
    query_grad, dk, dv, cross, copies = main_call(
        interpret, lax.axis_size("sp_0"), first, query_rows, key_rows, value_rows, output_grad, prior,
        gain_query, gain_key, table,
    )
    back = passed_along(cross, SP, -1)
    small = summed_copies(copies, "sp_0")
    small = spread_sum(small, ("sp_1", "sp_2"))
    gains = spread_sum(small[15:16], "tp")
    key_grad, value_grad = final_call(interpret, key_rows, dk, dv, back, gain_key)
    per_pair = small[:15].reshape(pairs, 5, LANES)
    tails = per_pair[:, 4].reshape(pairs, 2, HEAD)
    bias_grad = jnp.concatenate(
        [tails[:, :, 1:], per_pair[:, :4].reshape(pairs, 2, 2 * LANES), tails[:, :, :1]], axis=2
    ).reshape(heads, RSPAN)
    return query_grad, key_grad, value_grad, bias_grad, gains[0, :HEAD], gains[0, HEAD:]


def solution(mesh, sp_shape=(16, 8, 2), interpret=False):
    torus = Mesh(mesh.devices.reshape(*sp_shape, mesh.shape["tp"]), SP + ("tp",))
    placed = (P(SP, "tp"), P(SP, "tp"), P(SP, "tp"), P(), P(), P("tp", None), P(SP, "tp"))
    return jax.shard_map(
        functools.partial(body, interpret=interpret),
        mesh=torus,
        in_specs=placed,
        out_specs=(P(SP, "tp"), P(SP, "tp"), P(SP, "tp"), P("tp", None), P(), P()),
        check_vma=False,
    )
```

time: 356 us -> 96.3 us (0.27)
  the two profiles are of different devices: /device:TPU:24 before, /device:TPU:1 now
where the time goes in v1:
time: 96.3 us; the launch traced here: 95.8 us
  blocking collectives  27 us (28%)
  waiting for transfers between devices  22.2 us (23%)
  starting transfers between devices  21.5 us (22%)
  Pallas kernels  17.9 us (19%)
  local copies, waits for them, and re-layouts  4.58 us (5%)
  other arithmetic  1.77 us (2%)
    all_to_all x1, blocking collectives, summed_copies(): return jnp.sum(lax.all_to_all(copies, axes, 0, 0), axis=0)  27 us
    all_to_all x2, starting transfers between devices, summed_copies(): return jnp.sum(lax.all_to_all(copies, axes, 0, 0), axis=0)  15 us
    pallas_call x1, Pallas kernels, main_call(): pl.pallas_call(main_kernel, grid=(pairs,), in_specs=[pl.BlockSpec(memory_...  13.7 us
    ppermute x2, waiting for transfers between devices, passed_along(): return lax.ppermute(block, axis, route)  12.3 us
    all_to_all x2, waiting for transfers between devices, summed_copies(): return jnp.sum(lax.all_to_all(copies, axes, 0, 0), axis=0)  9.87 us
    ppermute x2, starting transfers between devices, passed_along(): return lax.ppermute(block, axis, route)  6.58 us
    pallas_call x1, Pallas kernels, final_call(): pl.pallas_call(final_kernel, grid=(width // LANES,), in_specs=[own, own,...  4.27 us
  transfers between devices with their start and end apart: 4, of which 3 were waited for; matrix products, arithmetic and copies ran while one was open for 3% of the time, Pallas kernels for 0%

profile of v1, /device:TPU:1, one launch (start us, length us, event | category | flops | bytes accessed | tf_op | source)
XLA Modules:
  0.0 95.8 jit_solution(5113847041029144011)
XLA Ops:
  0.6 0.0 slice-start.1
  0.6 0.0 slice-start
  0.7 0.0 copy-start.3
  0.7 1.0 %slice-done.1 = bf16[512,384]{1,0:T(8,128)(2,1)S(1)} async-done(((bf16[640,384]{1,0:T(8,128)(2,1)}), bf16[512,384]{1,0:T(8,128)(2,1)S(1)}, s32[]{:S(2)}) %slice-start.1) | async-done | bytes 393240 | tf_op jit(solution)/shard_map/slice | solution.py:349
  1.6 0.1 slice-done
  1.8 0.0 copy-start.6
  1.8 0.0 copy-start.7
  1.8 0.0 copy-start.8
  1.8 0.0 copy-start
  1.8 0.0 copy-start.1
  1.8 0.0 copy-start.2
  1.8 1.0 %pad_maximum_fusion = bf16[1024,384]{1,0:T(8,128)(2,1)} fusion(bf16[512,384]{1,0:T(8,128)(2,1)S(1)} %slice-done.1, bf16[512,384]{1,0:T(8,128)(2,1)S(1)} %slice-done), kind=kLoop, calls=%fused_computation | loop fusion | flops 1572864 | bytes 1572864 | tf_op jit(solution)/shard_map/concatenate | solution.py:349
  2.7 4.6 %collective-permute-start = (bf16[1024,384]{1,0:T(8,128)(2,1)}, bf16[1024,384]{1,0:T(8,128)(2,1)S(1)}, u32[]{:S(2)}, u32[]{:S(2)}) collective-permute-start(bf16[1024,384]{1,0:T(8,128)(2,1)} %pad_maximum_fusion), channel_id=1, source_target_pairs={{0,4},{4,8},{8,12},{12,16},{16,20},{20,24},{24,28},{28,32},{32,36}... | collective-permute-start | bytes 2359304 | tf_op jit(solution)/shard_map/ppermute | solution.py:334
  7.3 0.0 copy-done.6
  7.3 0.1 slice.48
  7.4 0.0 copy-done.7
  7.4 0.1 broadcast_in_dim_tile.6.query_gain_ref
  7.5 0.0 copy-done.8
  7.5 0.1 broadcast_in_dim_tile.7.key_gain_ref
  7.6 0.0 copy-start.4
  7.6 0.1 pad.4.clone
  7.7 0.1 pad_maximum_fusion.1
  7.8 12.3 %collective-permute-done.prior_key_ref.prior_value_ref = bf16[1024,384]{1,0:T(8,128)(2,1)S(1)} collective-permute-done((bf16[1024,384]{1,0:T(8,128)(2,1)}, bf16[1024,384]{1,0:T(8,128)(2,1)S(1)}, u32[]{:S(2)}, u32[]{:S(2)}) %collective-permute-start) | collective-permute-done | bytes 786464 | tf_op jit(solution)/shard_map/ppermute | solution.py:334
  20.1 0.0 copy-done.3
  20.1 0.0 copy-done
  20.1 0.0 copy-done.1
  20.1 0.0 copy-done.2
  20.1 13.7 %band_backward.1 = (bf16[640,384]{1,0:T(8,128)(2,1)}, f32[640,384]{1,0:T(8,128)}, f32[640,384]{1,0:T(8,128)}, bf16[1024,384]{1,0:T(8,128)(2,1)}, f32[16,16,128]{2,1,0:T(8,128)}) custom-call(f32[1]{0:T(128)} %bitcast.first_ref, bf16[640,384]{1,0:T(8,128)(2,1)S(1)} %copy-done.2, bf16[640,384]{1,0:T(8,128)(2,1)S(1)} %copy-done, bf16[640,384]{1,0:T(8,128)(2,1)S(1)} %copy-done.1, ...), custom_call_target="tpu_custom_call" | custom-call | tf_op jit(solution)/shard_map/band_backward/pallas_call | solution.py:278
  33.8 0.0 copy-done.4
  33.8 27.0 %all_to_all.15 = f32[16,16,128]{2,1,0:T(8,128)S(1)} all-to-all(f32[16,16,128]{2,1,0:T(8,128)} %get-tuple-element.19), channel_id=1, replica_groups=mesh['sp_0'=16,'sp_1'=8,'sp_2'=2,'tp'=4] {'sp_0'}, dimensions={0} | all-to-all | bytes 262144 | tf_op jit(solution)/shard_map/all_to_all | solution.py:342
  60.9 0.7 broadcast_in_dim.18
  61.5 10.9 %all-to-all-start.1 = ((f32[16,16,128]{2,1,0:T(8,128)}), f32[16,16,128]{2,1,0:T(8,128)S(1)}, u32[]{:S(2)}, u32[]{:S(2)}) async-start(f32[16,16,128]{2,1,0:T(8,128)} %broadcast_in_dim.18), calls=%async_computation.1 | async-start | bytes 262144 | tf_op jit(solution)/shard_map/all_to_all | solution.py:342
  72.5 2.0 %collective-permute-start.1 = (bf16[1024,384]{1,0:T(8,128)(2,1)}, bf16[1024,384]{1,0:T(8,128)(2,1)S(1)}, u32[]{:S(2)}, u32[]{:S(2)}) collective-permute-start(bf16[1024,384]{1,0:T(8,128)(2,1)} %get-tuple-element.16), channel_id=1, source_target_pairs={{4,0},{8,4},{12,8},{16,12},{20,16},{24,20},{28,24},{32,28},{36,32}... | collective-permute-start | bytes 2359304 | tf_op jit(solution)/shard_map/ppermute | solution.py:334
  74.5 6.9 %all-to-all-done.1 = f32[16,16,128]{2,1,0:T(8,128)S(1)} async-done(((f32[16,16,128]{2,1,0:T(8,128)}), f32[16,16,128]{2,1,0:T(8,128)S(1)}, u32[]{:S(2)}, u32[]{:S(2)}) %all-to-all-start.1) | async-done | bytes 131104 | tf_op jit(solution)/shard_map/all_to_all | solution.py:342
  81.4 0.6 broadcast_in_dim.20
  82.0 4.0 %all-to-all-start.2 = ((f32[4,1,128]{2,1,0:T(1,128)}), f32[4,1,128]{2,1,0:T(1,128)S(1)}, u32[]{:S(2)}, u32[]{:S(2)}) async-start(f32[4,1,128]{2,1,0:T(1,128)} %broadcast_in_dim.20), calls=%async_computation.2 | async-start | bytes 4096 | tf_op jit(solution)/shard_map/all_to_all | solution.py:342
  86.0 0.1 reshape_squeeze.3
  86.1 0.1 slice.52
  86.2 0.1 slice_reduce_fusion
  86.3 0.1 concatenate.22
  86.4 0.7 pad_maximum_fusion.2
  87.1 3.0 %all-to-all-done.2 = f32[4,1,128]{2,1,0:T(1,128)S(1)} async-done(((f32[4,1,128]{2,1,0:T(1,128)}), f32[4,1,128]{2,1,0:T(1,128)S(1)}, u32[]{:S(2)}, u32[]{:S(2)}) %all-to-all-start.2) | async-done | bytes 2080 | tf_op jit(solution)/shard_map/all_to_all | solution.py:342
  90.1 0.6 slice_bitcast_fusion.1
  90.7 0.0 collective-permute-done.1.back_key_ref.back_value_ref
  90.7 0.0 copy-start.5
  90.7 0.9 copy-done.5
  91.6 4.3 %key_and_value.1 = (bf16[640,384]{1,0:T(8,128)(2,1)}, bf16[640,384]{1,0:T(8,128)(2,1)}) custom-call(bf16[640,384]{1,0:T(8,128)(2,1)} %key_ref.3, f32[640,384]{1,0:T(8,128)} %get-tuple-element.14.dk_ref, f32[640,384]{1,0:T(8,128)} %get-tuple-element.15.dv_ref, bf16[1024,384]{1,0:T(8,128)(2,1)} %copy-done.5, bf16[1024,384]{1,0:T(8,128)(2,1)} %copy-done.5, ...), custom_call_target="tpu_custom_call" | custom-call | tf_op jit(solution)/shard_map/key_and_value/pallas_call | solution.py:320
  (14 shorter events, 0.1 us)
Async XLA Ops:
  0.6 1.0 %slice-start.1 = ((bf16[640,384]{1,0:T(8,128)(2,1)}), bf16[512,384]{1,0:T(8,128)(2,1)S(1)}, s32[]{:S(2)}) async-start(bf16[640,384]{1,0:T(8,128)(2,1)} %value_ref.1), calls=%async_computation.4 | async-start | bytes 786432 | tf_op jit(solution)/shard_map/slice | solution.py:349
  0.6 1.1 %slice-start = ((bf16[640,384]{1,0:T(8,128)(2,1)}), bf16[512,384]{1,0:T(8,128)(2,1)S(1)}, s32[]{:S(2)}) async-start(bf16[640,384]{1,0:T(8,128)(2,1)} %key_ref.3), calls=%async_computation.3 | async-start | bytes 786432 | tf_op jit(solution)/shard_map/slice | solution.py:349
  0.7 19.5 %copy-start.3 = (bf16[640,384]{1,0:T(8,128)(2,1)S(1)}, bf16[640,384]{1,0:T(8,128)(2,1)}, u32[]{:S(2)}) copy-start(bf16[640,384]{1,0:T(8,128)(2,1)} %grad_ref.1) | copy-start | bytes 1474564
  1.8 5.6 %copy-start.6 = (bf16[6,320]{1,0:T(8,128)(2,1)S(1)}, bf16[6,320]{1,0:T(8,128)(2,1)}, u32[]{:S(2)}) copy-start(bf16[6,320]{1,0:T(8,128)(2,1)} %param.12) | copy-start | bytes 11524
  1.8 5.7 %copy-start.7 = (bf16[64]{0:T(256)(128)(2,1)S(1)}, bf16[64]{0:T(256)(128)(2,1)}, u32[]{:S(2)}) copy-start(bf16[64]{0:T(256)(128)(2,1)} %param.10) | copy-start | bytes 388
  1.8 5.7 %copy-start.8 = (bf16[64]{0:T(256)(128)(2,1)S(1)}, bf16[64]{0:T(256)(128)(2,1)}, u32[]{:S(2)}) copy-start(bf16[64]{0:T(256)(128)(2,1)} %param.11) | copy-start | bytes 388
  1.8 18.4 %copy-start = (bf16[640,384]{1,0:T(8,128)(2,1)S(1)}, bf16[640,384]{1,0:T(8,128)(2,1)}, u32[]{:S(2)}) copy-start(bf16[640,384]{1,0:T(8,128)(2,1)} %key_ref.3) | copy-start | bytes 1474564
  1.8 18.4 %copy-start.1 = (bf16[640,384]{1,0:T(8,128)(2,1)S(1)}, bf16[640,384]{1,0:T(8,128)(2,1)}, u32[]{:S(2)}) copy-start(bf16[640,384]{1,0:T(8,128)(2,1)} %value_ref.1) | copy-start | bytes 1474564
  1.8 18.4 %copy-start.2 = (bf16[640,384]{1,0:T(8,128)(2,1)S(1)}, bf16[640,384]{1,0:T(8,128)(2,1)}, u32[]{:S(2)}) copy-start(bf16[640,384]{1,0:T(8,128)(2,1)} %query_ref.1) | copy-start | bytes 1474564
  2.7 17.4 %collective-permute-start = (bf16[1024,384]{1,0:T(8,128)(2,1)}, bf16[1024,384]{1,0:T(8,128)(2,1)S(1)}, u32[]{:S(2)}, u32[]{:S(2)}) collective-permute-start(bf16[1024,384]{1,0:T(8,128)(2,1)} %pad_maximum_fusion), channel_id=1, source_target_pairs={{0,4},{4,8},{8,12},{12,16},{16,20},{20,24},{24,28},{28,32},{32,36}... | collective-permute-start | bytes 2359304 | tf_op jit(solution)/shard_map/ppermute | solution.py:334
  7.6 26.2 %copy-start.4 = (f32[1,128]{1,0:T(1,128)}, f32[1,128]{1,0:T(1,128)S(1)}, u32[]{:S(2)}) copy-start(f32[1,128]{1,0:T(1,128)S(1)} %broadcast_in_dim_tile.7.key_gain_ref) | copy-start | bytes 1540
  61.5 19.8 %all-to-all-start.1 = ((f32[16,16,128]{2,1,0:T(8,128)}), f32[16,16,128]{2,1,0:T(8,128)S(1)}, u32[]{:S(2)}, u32[]{:S(2)}) async-start(f32[16,16,128]{2,1,0:T(8,128)} %broadcast_in_dim.18), calls=%async_computation.1 | async-start | bytes 262144 | tf_op jit(solution)/shard_map/all_to_all | solution.py:342
  72.5 18.2 %collective-permute-start.1 = (bf16[1024,384]{1,0:T(8,128)(2,1)}, bf16[1024,384]{1,0:T(8,128)(2,1)S(1)}, u32[]{:S(2)}, u32[]{:S(2)}) collective-permute-start(bf16[1024,384]{1,0:T(8,128)(2,1)} %get-tuple-element.16), channel_id=1, source_target_pairs={{4,0},{8,4},{12,8},{16,12},{20,16},{24,20},{28,24},{32,28},{36,32}... | collective-permute-start | bytes 2359304 | tf_op jit(solution)/shard_map/ppermute | solution.py:334
  82.0 8.1 %all-to-all-start.2 = ((f32[4,1,128]{2,1,0:T(1,128)}), f32[4,1,128]{2,1,0:T(1,128)S(1)}, u32[]{:S(2)}, u32[]{:S(2)}) async-start(f32[4,1,128]{2,1,0:T(1,128)} %broadcast_in_dim.20), calls=%async_computation.2 | async-start | bytes 4096 | tf_op jit(solution)/shard_map/all_to_all | solution.py:342
  90.7 0.9 copy-start.5

commit v2 on v1

v2 whole, which is shorter than its diff:
```python
import functools

import jax
import jax.numpy as jnp
from jax import lax
from jax.experimental import pallas as pl
from jax.experimental.pallas import tpu as pltpu
from jax.sharding import Mesh
from jax.sharding import PartitionSpec as P


SEG = 64
LEFT = 8
HEAD = 64
LANES = 128
RSPAN = 320
REACH = LEFT * SEG
NORM_EPS = 1e-06
HIDDEN = -1e30
LOCAL_MIB, MAIN_MIB, VALUE_MIB = 14, 18, 14
SP = ("sp_0", "sp_1", "sp_2")
F32 = jnp.float32
BF16 = jnp.bfloat16


def iota(shape, dim):
    return lax.broadcasted_iota(jnp.int32, shape, dim)


def dot(left, right, contract):
    return lax.dot_general(left, right, (contract, ((), ())), preferred_element_type=F32)


def half_means(values):
    same_half = (iota((2 * LANES, LANES), 0) % LANES) // HEAD == iota((2 * LANES, LANES), 1) // HEAD
    weights = jnp.where(same_half, 1.0 / HEAD, 0.0).astype(BF16)
    high = values.astype(BF16)
    low = (values - high.astype(F32)).astype(BF16)
    return dot(jnp.concatenate([high, low], axis=1), weights, ((1,), (0,)))


def normed(rows):
    widened = rows.astype(F32)
    scale = lax.rsqrt(half_means(widened * widened) + NORM_EPS)
    return widened * scale, scale


def by_head(rows):
    first = iota(rows.shape, 1) < HEAD
    zero = jnp.zeros_like(rows)
    return jnp.concatenate([jnp.where(first, rows, zero), jnp.where(first, zero, rows)], axis=0)


def fold(values, combine):
    return combine(values.reshape(-1, 8, values.shape[-1]), axis=0)


def toeplitz(row):
    top = pltpu.roll(jnp.broadcast_to(row, (8, LANES)), 0, 1, stride=1, stride_axis=0)
    return jnp.concatenate([top] + [pltpu.roll(top, 8 * i, 1) for i in range(1, 16)], axis=0)


def diagonal_sums(tile):
    rows = tile.shape[0]
    while rows > 8:
        rows //= 2
        tile = tile[:rows] + pltpu.roll(tile[rows:], LANES - rows, 1)
    for step in (4, 2, 1):
        tile = tile + pltpu.roll(pltpu.roll(tile, LANES - step, 1), 8 - step, 0)
    return tile[:1]


def norm_queries(rows, gain, hat_ref, scale_ref, two_ref):
    hat, scale = normed(rows)
    hat_ref[...] = hat
    scale_ref[...] = scale
    split_heads((hat * gain).astype(BF16) * jnp.asarray(HEAD**-0.5, BF16), two_ref)


def split_heads(rows, two_ref):
    for m in range(rows.shape[0] // LANES):
        two_ref[2 * m * LANES : 2 * (m + 1) * LANES] = by_head(rows[m * LANES : (m + 1) * LANES])


def norm_keys(rows, gain):
    hat, _ = normed(rows)
    unit = (hat * gain).astype(BF16)
    return hat, unit, (unit * jnp.asarray(HEAD**-0.5, BF16)).T


def write_bias(table_ref, bias_ref):
    square = (LANES, LANES)
    after = iota(square, 1) >= iota(square, 0)
    upper = iota(square, 0) < HEAD
    left = iota(square, 1) < HEAD
    for head in range(2):
        lanes = slice(head * LANES, (head + 1) * LANES)
        table = table_ref[0, head : head + 1]
        far = jnp.broadcast_to(table[:, :1], square)
        near = toeplitz(table[:, :LANES])
        middle = toeplitz(table[:, LANES : 2 * LANES])
        outer = toeplitz(table[:, 2 * LANES :])
        bias_ref[0:LANES, lanes] = jnp.where(upper & ~left, HIDDEN, far)
        bias_ref[LANES : 2 * LANES, lanes] = far
        bias_ref[2 * LANES : 3 * LANES, lanes] = jnp.where(after, far, outer)
        bias_ref[3 * LANES : 4 * LANES, lanes] = jnp.where(after, outer, middle)
        bias_ref[4 * LANES : 5 * LANES, lanes] = jnp.where(
            ~upper & left, HIDDEN, jnp.where(after, middle, near)
        )


def local_blocks():
    return [(m, b) for m in range(4) for b in range(4 - m, 5)]


def rows_at(index, size=LANES):
    return slice(index * size, (index + 1) * size)


def sweep(blocks, base, score_block, read_block, keep, far_sum, old_sum, between, following):
    s_ref, keep_weights, d_low_ref, d_sum_ref = keep
    peaks = {}

    def key_rows(j):
        return rows_at(j - base)

    def ahead(m, b):
        if m in blocks:
            top = score_block(m, b)
            if top is not None:
                peaks[m] = jnp.maximum(peaks[m], top) if m in peaks else top

    for b in range(5):
        ahead(blocks[0], b)
    for m in blocks:
        cols = rows_at(m - blocks[0], 2 * LANES)
        peak = jnp.max(peaks[m], axis=0, keepdims=True)
        total = jnp.zeros((8, 2 * LANES), F32)
        delta = jnp.zeros((8, 2 * LANES), F32)
        for b in range(5):
            scores, d_weights = read_block(m, b)
            raised = jnp.exp(scores - peak)
            s_ref[m % 2, rows_at(b)] = raised
            total = total + fold(raised, jnp.sum)
            delta = delta + fold(raised * d_weights, jnp.sum)
            ahead(m + 1, b)
        inverse = 1.0 / jnp.sum(total, axis=0, keepdims=True)
        delta = jnp.sum(delta, axis=0, keepdims=True) * inverse
        between(m)
        for b in range(5):
            weights = s_ref[m % 2, rows_at(b)] * inverse
            d_scores = weights * (read_block(m, b)[1] - delta)
            keep_weights(m, b, weights.astype(BF16))
            d_low_ref[key_rows(m + b), cols] = d_scores.astype(BF16)
            if b < 2:
                far_sum = far_sum + fold(d_scores, jnp.sum)
            else:
                kept_rows = rows_at(b - 2)
                if m > blocks[0]:
                    d_scores = d_sum_ref[kept_rows] + d_scores
                elif old_sum is not None:
                    d_scores = old_sum[kept_rows] + d_scores
                d_sum_ref[kept_rows] = d_scores
        following(m)
    return far_sum


def query_of(dq_t):
    return jnp.where(iota((LANES, LANES), 0) < HEAD, dq_t[:, :LANES], dq_t[:, LANES:]).T


def unnormed(grad, hat, scale, gain):
    scaled = grad * gain
    return (scale * (scaled - hat * half_means(scaled * hat))).astype(BF16)


def local_kernel(
    query_ref, key_ref, value_ref, grad_ref, query_gain_ref, key_gain_ref, table_ref,
    q_hat_out, q_two_out, g_two_out, k_hat_out, k_t_out, bias_out, d_sum_out, part_out,
    dk_out, s_out, dp_out, peak_out, q_scale_ref, dv_ref, query_grad_ref,
    k_ref, s_ref, dp_ref, w_low_ref, d_low_ref,
):
    last = query_ref.shape[0] // LANES - 1
    pair = pl.program_id(0)
    q_hat_ref, q_two_ref, g_two_ref, k_t_ref, bias_ref, s_local_ref, dp_local_ref = (
        ref.at[pair] for ref in (q_hat_out, q_two_out, g_two_out, k_t_out, bias_out, s_out, dp_out)
    )
    norm_queries(query_ref[...], query_gain_ref[...], q_hat_ref, q_scale_ref, q_two_ref)
    split_heads(grad_ref[...], g_two_ref)
    k_hat_out[pair], k_ref[...], k_t_ref[...] = norm_keys(key_ref[...], key_gain_ref[...])
    write_bias(table_ref, bias_ref)

    def products(m, b):
        keys = rows_at(m + b - 4)
        two = rows_at(m, 2 * LANES)
        scores = dot(k_ref[keys], q_two_ref[two], ((1,), (1,))) + bias_ref[rows_at(b)]
        return scores, dot(value_ref[keys], g_two_ref[two], ((1,), (1,)))

    def score_block(m, b):
        s_ref[m % 2, rows_at(b)], dp_ref[rows_at(b)] = scores, _ = products(m, b)
        return fold(scores, jnp.max)

    def keep_weights(m, b, weights):
        w_low_ref[rows_at(b)] = weights

    own = rows_at(last, 2 * LANES)
    far_sum = sweep(
        [last], 4, score_block, lambda m, b: (s_ref[m % 2, rows_at(b)], dp_ref[rows_at(b)]),
        (s_ref, keep_weights, d_low_ref, d_sum_out.at[pair]),
        jnp.zeros((8, 2 * LANES), F32), None, lambda m: None, lambda m: None,
    )
    here = rows_at(last)
    dq = query_of(dot(k_t_ref[...], d_low_ref[...], ((1,), (0,))))
    q_hat = q_hat_ref[here]
    query_grad_ref[...] = unnormed(dq, q_hat, q_scale_ref[here], query_gain_ref[...])
    part_out[pair, :, : 2 * LANES] = far_sum
    part_out[pair, :, 2 * LANES :] = fold(dq * q_hat, jnp.sum)
    dk_out[pair] = dot(d_low_ref[...], q_two_ref[own], ((1,), (0,)))
    dv_ref[...] = dot(w_low_ref[...], g_two_ref[own], ((1,), (0,)))
    peaks = {}
    for i, (m, b) in enumerate(local_blocks()):
        s_local_ref[rows_at(i)], dp_local_ref[rows_at(i)] = scores, _ = products(m, b)
        top = fold(scores, jnp.max)
        peaks[m] = jnp.maximum(peaks[m], top) if m in peaks else top
    for m, top in peaks.items():
        peak_out[pair, rows_at(m, 8)] = top


def main_kernel(
    first_ref, prior_ref, key_gain_ref,
    q_hat_in, q_two_in, g_two_in, k_hat_in, k_t_in, bias_in, d_sum_in, part_in, dk_in, s_in, dp_in, peak_in,
    dq_ref, w_low_ref, cross_ref, dk_ref, copies_ref,
    k_hat_prior, k_prior, k_t_prior, s_ref, dp_ref, d_low_ref, d_sum_ref, small_ref,
):
    count = dq_ref.shape[0] // LANES
    pair = pl.program_id(0)
    lanes_of_pair = pl.ds(pl.multiple_of(pair * LANES, LANES), LANES)
    q_hat_ref, q_two_ref, g_two_ref, own_hat_ref, bias_ref, s_local_ref, dp_local_ref = (
        ref.at[pair] for ref in (q_hat_in, q_two_in, g_two_in, k_hat_in, bias_in, s_in, dp_in)
    )
    index_of = {block: i for i, block in enumerate(local_blocks())}

    @pl.when(pair == 0)
    def _():
        for p in range(k_prior.shape[0]):
            k_hat_prior[p], k_prior[p], k_t_prior[p] = norm_keys(
                prior_ref[:REACH, p * LANES : (p + 1) * LANES], key_gain_ref[...]
            )

    k_ref, k_t_ref = k_prior.at[pair], k_t_prior.at[pair]
    gain_sums = [part_in[pair, :, 2 * LANES :], jnp.zeros((8, LANES), F32)]

    def score_block(m, b):
        if (m, b) in index_of:
            return peak_in[pair, rows_at(m, 8)] if b == 4 else None
        two = rows_at(m, 2 * LANES)
        scores = dot(k_ref[rows_at(m + b)], q_two_ref[two], ((1,), (1,))) + bias_ref[rows_at(b)] + first_ref[0]
        s_ref[m % 2, rows_at(b)] = scores
        values = prior_ref[REACH + (m + b) * LANES : REACH + (m + b + 1) * LANES, lanes_of_pair]
        dp_ref[m % 2, rows_at(b)] = dot(values, g_two_ref[two], ((1,), (1,)))
        return fold(scores, jnp.max)

    def read_block(m, b):
        if (m, b) in index_of:
            rows = rows_at(index_of[m, b])
            return s_local_ref[rows], dp_local_ref[rows]
        return s_ref[m % 2, rows_at(b)], dp_ref[m % 2, rows_at(b)]

    def keep_weights(m, b, weights):
        w_low_ref[rows_at(5 * m + b)] = weights

    def finish_query(m):
        if m < 0:
            return
        at = m * LANES
        cols = rows_at(m, 2 * LANES)
        dq_t = dot(k_t_ref[:, at:], d_low_ref[at:REACH, cols], ((1,), (0,)))
        dq_t = dq_t + dot(
            k_t_in[pair, :, : at + LANES], d_low_ref[REACH : REACH + at + LANES, cols], ((1,), (0,))
        )
        dq = query_of(dq_t)
        dq_ref[rows_at(m)] = dq
        gain_sums[0] = gain_sums[0] + fold(dq * q_hat_ref[rows_at(m)], jnp.sum)

    def key_side(j, low, high):
        cols = slice(2 * low * LANES, 2 * high * LANES)
        return dot(d_low_ref[rows_at(j), cols], q_two_ref[cols], ((1,), (0,)))

    def finish_keys(m):
        dk_low = key_side(m, 0, m + 1).astype(BF16)
        cross_ref[rows_at(m)] = dk_low
        gain_sums[1] = gain_sums[1] + fold(dk_low.astype(F32) * k_hat_prior[pair, rows_at(m)], jnp.sum)

    far_sum = sweep(
        list(range(count)), 0, score_block, read_block, (s_ref, keep_weights, d_low_ref, d_sum_ref),
        part_in[pair, :, : 2 * LANES], d_sum_in.at[pair], lambda m: finish_query(m - 1), finish_keys,
    )
    finish_query(count - 1)
    for j in range(4, count + 5):
        here = rows_at(j - 4)
        dk = dk_in[pair, here]
        if j < count + 4:
            dk = dk + key_side(j, j - 4, count)
        dk_ref[here] = dk
        gain_sums[1] = gain_sums[1] + fold(dk * own_hat_ref[here], jnp.sum)

    square = (LANES, LANES)
    after = iota(square, 1) >= iota(square, 0)
    tails = []
    for head in range(2):
        lanes = rows_at(head)
        two, three, four = (d_sum_ref[rows_at(i), lanes] for i in range(3))
        zero = jnp.zeros(square, F32)
        far = far_sum[:, lanes] + fold(jnp.where(after, two, zero), jnp.sum)
        far = jnp.sum(jnp.sum(far, axis=0, keepdims=True), axis=1, keepdims=True)
        small_ref[pl.ds(5 * pair + 2 * head, 1)] = diagonal_sums(jnp.where(after, four, three))
        small_ref[pl.ds(5 * pair + 2 * head + 1, 1)] = diagonal_sums(jnp.where(after, three, two))
        tail = diagonal_sums(jnp.where(after, zero, four))
        tails.append(jnp.where(iota((1, LANES), 1) == HEAD, far, tail))
    first_half = iota((1, LANES), 1) < HEAD
    small_ref[pl.ds(5 * pair + 4, 1)] = jnp.where(first_half, pltpu.roll(tails[0], HEAD, 1), tails[1])
    both = []
    for part in gain_sums:
        part = jnp.sum(part, axis=0, keepdims=True)
        both.append(part + pltpu.roll(part, HEAD, 1))
    gains = jnp.where(first_half, both[0], both[1])

    @pl.when(pair == 0)
    def _():
        small_ref[15:16] = gains

    @pl.when(pair > 0)
    def _():
        small_ref[15:16] = small_ref[15:16] + gains

    @pl.when(pair == pl.num_programs(0) - 1)
    def _():
        rows = copies_ref.shape[1]
        for copy in range(copies_ref.shape[0]):
            start = copy * rows % 16
            copies_ref[copy] = small_ref[start : start + rows]


def value_kernel(
    query_gain_ref, g_two_in, q_hat_in, w_low_ref, dv_ref, dq_ref, q_scale_ref, dk_cross_ref, last_grad_ref,
    query_grad_ref, dv_out, cross_ref,
):
    pair = pl.program_id(0)
    count = dq_ref.shape[0] // LANES
    cross_ref[:REACH] = dk_cross_ref[...]
    for j in range(count + 5):
        seen = range(max(0, j - 4), min(count, j + 1))
        if seen:
            weights = jnp.concatenate([w_low_ref[rows_at(4 * m + j)] for m in seen], axis=1)
            grads = g_two_in[pair, 2 * seen.start * LANES : 2 * seen.stop * LANES]
            dv = dot(weights, grads, ((1,), (0,)))
        if j < 4:
            cross_ref[rows_at(4 + j)] = dv.astype(BF16)
        else:
            own = dv_ref[rows_at(j - 4)]
            dv_out[rows_at(j - 4)] = own + dv if seen else own
    for m in range(count):
        here = rows_at(m)
        query_grad_ref[here] = unnormed(dq_ref[here], q_hat_in[pair, here], q_scale_ref[here], query_gain_ref[...])
    query_grad_ref[rows_at(count)] = last_grad_ref[...]


def final_kernel(key_ref, dk_ref, dv_ref, back_key_ref, back_value_ref, key_gain_ref, key_grad_ref, value_grad_ref):
    tokens = key_ref.shape[0]
    own = tokens - REACH
    for start, count in ((0, own), (own, REACH)):
        rows = slice(start, start + count)
        dk = dk_ref[rows]
        dv = dv_ref[rows]
        if start:
            dk = dk + back_key_ref[...].astype(F32)
            dv = dv + back_value_ref[...].astype(F32)
        value_grad_ref[rows] = dv.astype(BF16)
        k_hat, k_scale = normed(key_ref[rows])
        scaled = dk * key_gain_ref[...]
        mean = half_means(scaled * k_hat)
        key_grad_ref[rows] = (k_scale * (scaled - k_hat * mean)).astype(BF16)


def columns(rows, block=0):
    return pl.BlockSpec((rows, LANES), lambda p: (block, p))


def fixed(shape):
    return pl.BlockSpec(shape, lambda p: (0,) * len(shape))


def params(interpret, mebibytes):
    return None if interpret else pltpu.CompilerParams(vmem_limit_bytes=mebibytes * 2**20)


def in_vmem():
    return pl.BlockSpec(memory_space=pltpu.VMEM)


def local_call(interpret, query, key, value, grad, query_gain, key_gain, table):
    tokens, width = query.shape
    pairs = width // LANES
    own = columns(tokens)
    vmem = jax.ShapeDtypeStruct if interpret else pltpu.VMEM
    wide = 2 * LANES
    found = LANES * len(local_blocks())
    shapes = {
        "q_hat": ((tokens, LANES), F32),
        "q_two": ((2 * tokens, LANES), BF16),
        "g_two": ((2 * tokens, LANES), BF16),
        "k_hat": ((tokens, LANES), F32),
        "k_t": ((LANES, tokens), BF16),
        "bias": ((5 * LANES, wide), F32),
        "d_sum": ((3 * LANES, wide), F32),
        "part": ((8, 3 * LANES), F32),
        "dk": ((tokens, LANES), F32),
        "scores": ((found, wide), F32),
        "d_weights": ((found, wide), F32),
        "peaks": ((4 * 8, wide), F32),
    }
    hbm = jax.ShapeDtypeStruct if interpret else pltpu.HBM
    *arrays, q_scale, dv, last_grad = pl.pallas_call(
        local_kernel,
        grid=(pairs,),
        in_specs=[
            own, own, own, own, fixed((1, LANES)), fixed((1, LANES)),
            pl.BlockSpec((1, 2, 3 * LANES), lambda p: (p, 0, 0)),
        ],
        out_specs=[in_vmem()] * len(shapes) + [own, own, columns(LANES)],
        out_shape=[vmem((pairs,) + shape, dtype) for shape, dtype in shapes.values()]
        + [hbm((tokens, width), F32), hbm((tokens, width), F32), hbm((LANES, width), BF16)],
        scratch_shapes=[
            pltpu.VMEM((tokens, LANES), BF16),
            pltpu.VMEM((2, 5 * LANES, wide), F32),
            pltpu.VMEM((5 * LANES, wide), F32),
            pltpu.VMEM((5 * LANES, wide), BF16),
            pltpu.VMEM((5 * LANES, wide), BF16),
        ],
        compiler_params=params(interpret, LOCAL_MIB),
        interpret=interpret,
        name="local_backward",
    )(query, key, value, grad, query_gain, key_gain, table)
    return dict(zip(shapes, arrays)), (dv, q_scale, last_grad)


def weights_block(early):
    return pl.BlockSpec((None, 5 * early, 2 * LANES), lambda p: (p, 0, 0))


def main_call(interpret, far, halves, first, prior, key_gain, local):
    pairs, tokens = local["q_hat"].shape[:2]
    width = pairs * LANES
    extended = tokens + REACH
    early = tokens - LANES
    wide = 2 * LANES
    hbm = jax.ShapeDtypeStruct if interpret else pltpu.HBM
    copies = (far * halves, 16 // halves, LANES)
    taken = (
        "q_hat", "q_two", "g_two", "k_hat", "k_t", "bias", "d_sum", "part", "dk", "scores", "d_weights", "peaks",
    )
    return pl.pallas_call(
        main_kernel,
        grid=(pairs,),
        in_specs=[pl.BlockSpec(memory_space=pltpu.SMEM), in_vmem(), fixed((1, LANES))] + [in_vmem()] * len(taken),
        out_specs=[
            columns(early), weights_block(early), columns(REACH), columns(tokens), fixed(copies),
        ],
        out_shape=[
            hbm((early, width), F32),
            hbm((pairs, 5 * early, wide), BF16),
            hbm((REACH, width), BF16),
            hbm((tokens, width), F32),
            hbm(copies, F32),
        ],
        scratch_shapes=[
            pltpu.VMEM((pairs, REACH, LANES), F32),
            pltpu.VMEM((pairs, REACH, LANES), BF16),
            pltpu.VMEM((pairs, LANES, REACH), BF16),
            pltpu.VMEM((2, 5 * LANES, wide), F32),
            pltpu.VMEM((2, 5 * LANES, wide), F32),
            pltpu.VMEM((extended, 2 * early), BF16),
            pltpu.VMEM((3 * LANES, wide), F32),
            pltpu.VMEM((16, LANES), F32),
        ],
        compiler_params=params(interpret, MAIN_MIB),
        interpret=interpret,
        name="band_backward",
    )(first, prior, key_gain, *(local[name] for name in taken))


def value_call(interpret, query_gain, local, w_low, dv, dq, q_scale, dk_cross, last_grad):
    tokens, width = dv.shape
    early = dq.shape[0]
    hbm = jax.ShapeDtypeStruct if interpret else pltpu.HBM
    own = columns(tokens)
    return pl.pallas_call(
        value_kernel,
        grid=(width // LANES,),
        in_specs=[
            fixed((1, LANES)), in_vmem(), in_vmem(),
            weights_block(early), own, columns(early), own, columns(REACH), columns(LANES),
        ],
        out_specs=[own, own, columns(2 * REACH)],
        out_shape=[
            hbm((tokens, width), BF16),
            hbm((tokens, width), F32),
            hbm((2 * REACH, width), BF16),
        ],
        compiler_params=params(interpret, VALUE_MIB),
        interpret=interpret,
        name="value_backward",
    )(query_gain, local["g_two"], local["q_hat"], w_low, dv, dq, q_scale, dk_cross, last_grad)


def final_call(interpret, key, dk, dv, back, key_gain):
    tokens, width = key.shape
    own = columns(tokens)
    return pl.pallas_call(
        final_kernel,
        grid=(width // LANES,),
        in_specs=[own, own, own, columns(REACH), columns(REACH, 1), fixed((1, LANES))],
        out_specs=[own, own],
        out_shape=[jax.ShapeDtypeStruct((tokens, width), BF16)] * 2,
        interpret=interpret,
        name="key_and_value",
    )(key, dk, dv, back, back, key_gain)


def passed_along(block, axis, distance):
    devices = range(lax.axis_size(axis))
    route = [(i - distance, i) for i in devices if i - distance in devices]
    return lax.ppermute(block, axis, route)


def body(query_rows, key_rows, value_rows, query_gain, key_gain, position_bias, output_grad, interpret=False):
    tokens = query_rows.shape[0]
    heads = position_bias.shape[0]
    pairs = heads // 2
    gain_query = jnp.tile(query_gain.astype(F32), 2)[None]
    gain_key = jnp.tile(key_gain.astype(F32), 2)[None]
    table = position_bias.astype(F32)
    table = jnp.concatenate(
        [table[:, -1:], jnp.zeros((heads, 3 * LANES - RSPAN), F32), table[:, :-1]], axis=1
    ).reshape(pairs, 2, 3 * LANES)
    far, near, halves = (lax.axis_size(axis) for axis in SP)
    groups = lax.axis_size("tp")
    first = jnp.where(lax.axis_index(SP) == 0, HIDDEN, 0.0).astype(F32).reshape(1)
    sent = jnp.concatenate([key_rows[tokens - REACH :], value_rows[tokens - REACH :]], axis=0)
    prior = passed_along(sent, SP, 1)
    local, (dv, q_scale, last_grad) = local_call(
        interpret, query_rows, key_rows, value_rows, output_grad, gain_query, gain_key, table
    )
    dq, w_low, dk_cross, dk, copies = main_call(interpret, far, halves, first, prior, gain_key, local)
    query_grad, dv, cross = value_call(interpret, gain_query, local, w_low, dv, dq, q_scale, dk_cross, last_grad)
    back = passed_along(cross, SP, -1)
    half = jnp.sum(lax.all_to_all(copies, ("sp_0", "sp_2"), 0, 0), axis=0)
    spread = jnp.broadcast_to(half[None], (near * halves * groups,) + half.shape)
    spread = lax.all_to_all(spread, ("sp_1", "sp_2", "tp"), 0, 0)
    spread = jnp.sum(spread.reshape((near, halves, groups) + half.shape), axis=0)
    key_grad, value_grad = final_call(interpret, key_rows, dk, dv, back, gain_key)
    gains = jnp.sum(spread[-1, :, -1], axis=0)
    small = lax.dynamic_index_in_dim(spread, lax.axis_index("tp"), 1, keepdims=False).reshape(16, LANES)
    per_pair = small[:15].reshape(pairs, 5, LANES)
    tails = per_pair[:, 4].reshape(pairs, 2, HEAD)
    bias_grad = jnp.concatenate(
        [tails[:, :, 1:], per_pair[:, :4].reshape(pairs, 2, 2 * LANES), tails[:, :, :1]], axis=2
    ).reshape(heads, RSPAN)
    return query_grad, key_grad, value_grad, bias_grad, gains[:HEAD], gains[HEAD:]


def solution(mesh, sp_shape=(16, 8, 2), interpret=False):
    torus = Mesh(mesh.devices.reshape(*sp_shape, mesh.shape["tp"]), SP + ("tp",))
    placed = (P(SP, "tp"), P(SP, "tp"), P(SP, "tp"), P(), P(), P("tp", None), P(SP, "tp"))
    return jax.shard_map(
        functools.partial(body, interpret=interpret),
        mesh=torus,
        in_specs=placed,
        out_specs=(P(SP, "tp"), P(SP, "tp"), P(SP, "tp"), P("tp", None), P(), P()),
        check_vma=False,
    )
```

time: 96.3 us -> 91.8 us (0.953)
  blocking collectives: 27 us -> 0 us
  starting transfers between devices: 21.5 us -> 36.1 us
  local copies, waits for them, and re-layouts: 4.58 us -> 11.6 us
  Pallas kernels: 17.9 us -> 24 us
  waiting for transfers between devices: 22.2 us -> 16.8 us
    all_to_all x1 -> x0, blocking collectives: 27 us -> none  [summed_copies(): return jnp.sum(lax.all_to_all(copies, axes, 0, 0), axis=0)]
    all_to_all x2, starting transfers between devices: 15 us -> 29.4 us  [the longest x1 19.8 us: body(): half = jnp.sum(lax.all_to_all(copies, ('sp_0', 'sp_2'), 0, 0), axis=0)]
    pallas_call x0 -> x2, Pallas kernels: none -> 9.94 us  [the longest x1 6.9 us: local_call(): pl.pallas_call(local_kernel, grid=(pairs,), in_specs=[own, own, own, own,...]
    ppermute x2, waiting for transfers between devices: 12.3 us -> 4.5 us  [passed_along(): return lax.ppermute(block, axis, route)]
    unnamed x18 -> x30, local copies, waits for them, and re-layouts: 0.94 us -> 7.41 us
    pallas_call x1, Pallas kernels: 13.7 us -> 9.79 us  [main_call(): pl.pallas_call(main_kernel, grid=(pairs,), in_specs=[pl.BlockSpec(memory_...]
    all_to_all x2, waiting for transfers between devices: 9.87 us -> 12.3 us  [the longest x1 7.07 us: body(): spread = lax.all_to_all(spread, ('sp_1', 'sp_2', 'tp'), 0, 0)]
  transfers between devices with their start and end apart: 4 -> 4, of which waited for: 3 -> 3; matrix products, arithmetic and copies ran while one was open for 3% -> 1% of each run, Pallas kernels for 0% -> 16%
where the time goes in v2:
time: 91.8 us; the launch traced here: 91.2 us
  starting transfers between devices  36.1 us (39%)
  Pallas kernels  24 us (26%)
  waiting for transfers between devices  16.8 us (18%)
  local copies, waits for them, and re-layouts  11.6 us (13%)
  other arithmetic  1.8 us (2%)
    all_to_all x1, starting transfers between devices, body(): half = jnp.sum(lax.all_to_all(copies, ('sp_0', 'sp_2'), 0, 0), axis=0)  19.8 us
    pallas_call x1, Pallas kernels, main_call(): pl.pallas_call(main_kernel, grid=(pairs,), in_specs=[pl.BlockSpec(memory_...  9.79 us
    all_to_all x1, starting transfers between devices, body(): spread = lax.all_to_all(spread, ('sp_1', 'sp_2', 'tp'), 0, 0)  9.62 us
    unnamed x30, local copies, waits for them, and re-layouts  7.41 us
    all_to_all x1, waiting for transfers between devices, body(): spread = lax.all_to_all(spread, ('sp_1', 'sp_2', 'tp'), 0, 0)  7.07 us
    pallas_call x1, Pallas kernels, local_call(): pl.pallas_call(local_kernel, grid=(pairs,), in_specs=[own, own, own, own,...  6.9 us
    ppermute x2, starting transfers between devices, passed_along(): return lax.ppermute(block, axis, route)  6.71 us
    all_to_all x1, waiting for transfers between devices, body(): half = jnp.sum(lax.all_to_all(copies, ('sp_0', 'sp_2'), 0, 0), axis=0)  5.21 us
  transfers between devices with their start and end apart: 4, of which 3 were waited for; matrix products, arithmetic and copies ran while one was open for 1% of the time, Pallas kernels for 16%

profile of v2, /device:TPU:1, one launch (start us, length us, event | category | flops | bytes accessed | tf_op | source)
XLA Modules:
  0.0 91.2 jit_solution(10603846731220873216)
XLA Ops:
  0.6 0.0 copy-start.2
  0.6 0.0 copy-start.1
  0.7 0.0 copy-start.12
  0.7 0.0 copy-start.13
  0.7 0.0 copy-start.14
  0.7 0.0 copy-start.6
  0.7 1.1 %slice.39 = bf16[512,384]{1,0:T(8,128)(2,1)S(1)} slice(bf16[640,384]{1,0:T(8,128)(2,1)} %value_ref.1), slice={[128:640], [0:384]} | slice | bytes 786432 | tf_op jit(solution)/shard_map/slice | solution.py:549
  1.8 1.0 %slice.38 = bf16[512,384]{1,0:T(8,128)(2,1)S(1)} slice(bf16[640,384]{1,0:T(8,128)(2,1)} %key_ref.3), slice={[128:640], [0:384]} | slice | bytes 786432 | tf_op jit(solution)/shard_map/slice | solution.py:549
  2.9 1.0 %pad_maximum_fusion = bf16[1024,384]{1,0:T(8,128)(2,1)} fusion(bf16[512,384]{1,0:T(8,128)(2,1)S(1)} %slice.39, bf16[512,384]{1,0:T(8,128)(2,1)S(1)} %slice.38), kind=kLoop, calls=%fused_computation | loop fusion | flops 1572864 | bytes 1572864 | tf_op jit(solution)/shard_map/concatenate | solution.py:549
  3.9 4.6 %collective-permute-start = (bf16[1024,384]{1,0:T(8,128)(2,1)}, bf16[1024,384]{1,0:T(8,128)(2,1)}, u32[]{:S(2)}, u32[]{:S(2)}) collective-permute-start(bf16[1024,384]{1,0:T(8,128)(2,1)} %pad_maximum_fusion), channel_id=1, source_target_pairs={{0,4},{4,8},{8,12},{12,16},{16,20},{20,24},{24,28},{28,32},{32,36}... | collective-permute-start | bytes 2359304 | tf_op jit(solution)/shard_map/ppermute | solution.py:533
  8.4 0.0 copy-done.12
  8.4 0.1 slice.48
  8.5 0.0 copy-done.13
  8.5 0.1 broadcast_in_dim_tile.6.query_gain_ref
  8.6 0.0 copy-done.14
  8.6 0.1 broadcast_in_dim_tile.7.key_gain_ref
  8.7 0.0 copy-start.10
  8.7 0.1 pad.6.clone
  8.8 0.1 pad_maximum_fusion.1
  8.9 0.0 copy-done.2
  8.9 0.0 copy-done.1
  8.9 0.0 copy-done.6
  8.9 0.0 copy-start.7
  8.9 1.0 %copy-done.7 = bf16[640,384]{1,0:T(8,128)(2,1)S(1)} copy-done((bf16[640,384]{1,0:T(8,128)(2,1)S(1)}, bf16[640,384]{1,0:T(8,128)(2,1)}, u32[]{:S(2)}) %copy-start.7) | copy-done | bytes 491544
  10.0 6.9 %local_backward.1 = (f32[3,640,128]{2,1,0:T(8,128)S(1)}, bf16[3,1280,128]{2,1,0:T(8,128)(2,1)S(1)}, bf16[3,1280,128]{2,1,0:T(8,128)(2,1)S(1)}, f32[3,640,128]{2,...) custom-call(bf16[640,384]{1,0:T(8,128)(2,1)S(1)} %copy-done.6, ...), custom_call_target="tpu_custom_call" | custom-call | tf_op jit(solution)/shard_map/local_backward/pallas_call | solution.py:423
  16.9 4.5 %collective-permute-done.prior_ref = bf16[1024,384]{1,0:T(8,128)(2,1)} collective-permute-done((bf16[1024,384]{1,0:T(8,128)(2,1)}, bf16[1024,384]{1,0:T(8,128)(2,1)}, u32[]{:S(2)}, u32[]{:S(2)}) %collective-permute-start) | collective-permute-done | bytes 786464 | tf_op jit(solution)/shard_map/ppermute | solution.py:533
  21.4 0.0 copy-start.3
  21.4 0.0 copy-start.9
  21.4 9.8 %band_backward.1 = (f32[512,384]{1,0:T(8,128)}, bf16[3,2560,256]{2,1,0:T(8,128)(2,1)}, bf16[512,384]{1,0:T(8,128)(2,1)}, f32[640,384]{1,0:T(8,128)}, f32[32,8,128]{2,1,0:T(8,128)}) custom-call(f32[1]{0:T(128)} %bitcast.first_ref, bf16[1024,384]{1,0:T(8,128)(2,1)} %collective-permute-done.prior_ref, f32[1,128]{1,0:T(1,128)S(1)} %broadcast_in_dim_tile.7.key_gain_ref, ...), custom_call_target="tpu_custom_call" | custom-call | tf_op jit(solution)/shard_map/band_backward/pallas_call | solution.py:462
  31.1 0.0 copy-done.10
  31.2 19.8 %all-to-all-start = ((f32[32,8,128]{2,1,0:T(8,128)}), f32[32,8,128]{2,1,0:T(8,128)S(1)}, u32[]{:S(2)}, u32[]{:S(2)}) async-start(f32[32,8,128]{2,1,0:T(8,128)} %get-tuple-element.55), calls=%async_computation | async-start | bytes 262144 | tf_op jit(solution)/shard_map/all_to_all | solution.py:557
  51.0 0.0 copy-done.3
  51.0 0.0 copy-done.9
  51.0 0.0 copy-start
  51.0 2.1 %copy-done = bf16[3,2560,256]{2,1,0:T(8,128)(2,1)S(1)} copy-done((bf16[3,2560,256]{2,1,0:T(8,128)(2,1)S(1)}, bf16[3,2560,256]{2,1,0:T(8,128)(2,1)}, u32[]{:S(2)}) %copy-start) | copy-done | bytes 3932184
  53.1 0.0 copy-start.4
  53.1 1.2 %copy-done.4 = f32[640,384]{1,0:T(8,128)S(1)} copy-done((f32[640,384]{1,0:T(8,128)S(1)}, f32[640,384]{1,0:T(8,128)}, u32[]{:S(2)}) %copy-start.4) | copy-done | bytes 983064
  54.3 0.0 copy-start.5
  54.3 1.1 %copy-done.5 = f32[512,384]{1,0:T(8,128)S(1)} copy-done((f32[512,384]{1,0:T(8,128)S(1)}, f32[512,384]{1,0:T(8,128)}, u32[]{:S(2)}) %copy-start.5) | copy-done | bytes 786456
  55.5 0.0 copy-start.8
  55.5 1.0 %copy-done.8 = bf16[512,384]{1,0:T(8,128)(2,1)S(1)} copy-done((bf16[512,384]{1,0:T(8,128)(2,1)S(1)}, bf16[512,384]{1,0:T(8,128)(2,1)}, u32[]{:S(2)}) %copy-start.8) | copy-done | bytes 393240
  56.4 3.0 %value_backward.1 = (bf16[640,384]{1,0:T(8,128)(2,1)}, f32[640,384]{1,0:T(8,128)}, bf16[1024,384]{1,0:T(8,128)(2,1)}) custom-call(f32[1,128]{1,0:T(1,128)S(1)} %broadcast_in_dim_tile.6.query_gain_ref, bf16[3,1280,128]{2,1,0:T(8,128)(2,1)S(1)} %get-tuple-element.31.g_two_in, f32[3,640,128]{2,1,0:T(8,128)S(1)} %get-tuple-element.32.q_hat_in, ...), custom_call_target="tpu_custom_call" | custom-call | tf_op jit(solution)/shard_map/value_backward/pallas_call | solution.py:497
  59.5 2.1 %collective-permute-start.1 = (bf16[1024,384]{1,0:T(8,128)(2,1)}, bf16[1024,384]{1,0:T(8,128)(2,1)S(1)}, u32[]{:S(2)}, u32[]{:S(2)}) collective-permute-start(bf16[1024,384]{1,0:T(8,128)(2,1)} %get-tuple-element.52), channel_id=1, source_target_pairs={{4,0},{8,4},{12,8},{16,12},{20,16},{24,20},{28,24},{32,28},{36,32}... | collective-permute-start | bytes 2359304 | tf_op jit(solution)/shard_map/ppermute | solution.py:533
  61.6 5.2 %all-to-all-done = f32[32,8,128]{2,1,0:T(8,128)S(1)} async-done(((f32[32,8,128]{2,1,0:T(8,128)}), f32[32,8,128]{2,1,0:T(8,128)S(1)}, u32[]{:S(2)}, u32[]{:S(2)}) %all-to-all-start) | async-done | bytes 131104 | tf_op jit(solution)/shard_map/all_to_all | solution.py:557
  66.9 0.7 broadcast_in_dim.10
  67.6 9.6 %all-to-all-start.1 = ((f32[64,8,128]{2,1,0:T(8,128)}), f32[64,8,128]{2,1,0:T(8,128)S(1)}, u32[]{:S(2)}, u32[]{:S(2)}) async-start(f32[64,8,128]{2,1,0:T(8,128)} %broadcast_in_dim.10), calls=%async_computation.1 | async-start | bytes 524288 | tf_op jit(solution)/shard_map/all_to_all | solution.py:559
  77.2 0.0 collective-permute-done.1.back_key_ref.back_value_ref
  77.2 0.0 copy-start.11
  77.2 0.9 %copy-done.11 = bf16[1024,384]{1,0:T(8,128)(2,1)} copy-done((bf16[1024,384]{1,0:T(8,128)(2,1)}, bf16[1024,384]{1,0:T(8,128)(2,1)S(1)}, u32[]{:S(2)}) %copy-start.11) | copy-done | bytes 786456
  78.1 4.3 %key_and_value.1 = (bf16[640,384]{1,0:T(8,128)(2,1)}, bf16[640,384]{1,0:T(8,128)(2,1)}) custom-call(bf16[640,384]{1,0:T(8,128)(2,1)} %key_ref.3, f32[640,384]{1,0:T(8,128)} %get-tuple-element.50.dk_ref, f32[640,384]{1,0:T(8,128)} %get-tuple-element.51.dv_ref, bf16[1024,384]{1,0:T(8,128)(2,1)} %copy-done.11, bf16[1024,384]{1,0:T(8,128)(2,1)} %copy-done.11, ...), custom_call_target="tpu_custom_call" | custom-call | tf_op jit(solution)/shard_map/key_and_value/pallas_call | solution.py:519
  82.4 7.1 %all-to-all-done.1 = f32[64,8,128]{2,1,0:T(8,128)S(1)} async-done(((f32[64,8,128]{2,1,0:T(8,128)}), f32[64,8,128]{2,1,0:T(8,128)S(1)}, u32[]{:S(2)}, u32[]{:S(2)}) %all-to-all-start.1) | async-done | bytes 262176 | tf_op jit(solution)/shard_map/all_to_all | solution.py:559
  89.6 0.1 reshape_squeeze.3
  89.7 0.1 slice_reduce_fusion
  89.8 0.1 slice.52
  89.8 0.6 fusion
  90.4 0.1 concatenate.22
  90.5 0.7 pad_maximum_fusion.2
  (14 shorter events, 0.2 us)
Async XLA Ops:
  0.6 8.3 %copy-start.2 = (bf16[640,384]{1,0:T(8,128)(2,1)S(1)}, bf16[640,384]{1,0:T(8,128)(2,1)}, u32[]{:S(2)}) copy-start(bf16[640,384]{1,0:T(8,128)(2,1)} %value_ref.1) | copy-start | bytes 1474564
  0.6 8.3 %copy-start.1 = (bf16[640,384]{1,0:T(8,128)(2,1)S(1)}, bf16[640,384]{1,0:T(8,128)(2,1)}, u32[]{:S(2)}) copy-start(bf16[640,384]{1,0:T(8,128)(2,1)} %key_ref.3) | copy-start | bytes 1474564
  0.7 7.8 %copy-start.12 = (bf16[6,320]{1,0:T(8,128)(2,1)S(1)}, bf16[6,320]{1,0:T(8,128)(2,1)}, u32[]{:S(2)}) copy-start(bf16[6,320]{1,0:T(8,128)(2,1)} %param.12) | copy-start | bytes 11524
  0.7 7.9 %copy-start.13 = (bf16[64]{0:T(256)(128)(2,1)S(1)}, bf16[64]{0:T(256)(128)(2,1)}, u32[]{:S(2)}) copy-start(bf16[64]{0:T(256)(128)(2,1)} %param.10) | copy-start | bytes 388
  0.7 7.9 %copy-start.14 = (bf16[64]{0:T(256)(128)(2,1)S(1)}, bf16[64]{0:T(256)(128)(2,1)}, u32[]{:S(2)}) copy-start(bf16[64]{0:T(256)(128)(2,1)} %param.11) | copy-start | bytes 388
  0.7 8.2 %copy-start.6 = (bf16[640,384]{1,0:T(8,128)(2,1)S(1)}, bf16[640,384]{1,0:T(8,128)(2,1)}, u32[]{:S(2)}) copy-start(bf16[640,384]{1,0:T(8,128)(2,1)} %query_ref.1) | copy-start | bytes 1474564
  3.9 17.5 %collective-permute-start = (bf16[1024,384]{1,0:T(8,128)(2,1)}, bf16[1024,384]{1,0:T(8,128)(2,1)}, u32[]{:S(2)}, u32[]{:S(2)}) collective-permute-start(bf16[1024,384]{1,0:T(8,128)(2,1)} %pad_maximum_fusion), channel_id=1, source_target_pairs={{0,4},{4,8},{8,12},{12,16},{16,20},{20,24},{24,28},{28,32},{32,36}... | collective-permute-start | bytes 2359304 | tf_op jit(solution)/shard_map/ppermute | solution.py:533
  8.7 22.5 %copy-start.10 = (f32[1,128]{1,0:T(1,128)}, f32[1,128]{1,0:T(1,128)S(1)}, u32[]{:S(2)}) copy-start(f32[1,128]{1,0:T(1,128)S(1)} %broadcast_in_dim_tile.7.key_gain_ref) | copy-start | bytes 1540
  8.9 1.0 %copy-start.7 = (bf16[640,384]{1,0:T(8,128)(2,1)S(1)}, bf16[640,384]{1,0:T(8,128)(2,1)}, u32[]{:S(2)}) copy-start(bf16[640,384]{1,0:T(8,128)(2,1)} %grad_ref.1) | copy-start | bytes 1474564
  21.4 29.6 %copy-start.3 = (f32[640,384]{1,0:T(8,128)S(1)}, f32[640,384]{1,0:T(8,128)}, u32[]{:S(2)}) copy-start(f32[640,384]{1,0:T(8,128)} %get-tuple-element.46.q_scale_ref) | copy-start | bytes 2949124
  21.4 29.6 %copy-start.9 = (bf16[128,384]{1,0:T(8,128)(2,1)S(1)}, bf16[128,384]{1,0:T(8,128)(2,1)}, u32[]{:S(2)}) copy-start(bf16[128,384]{1,0:T(8,128)(2,1)} %get-tuple-element.48.last_grad_ref) | copy-start | bytes 294916
  31.2 35.7 %all-to-all-start = ((f32[32,8,128]{2,1,0:T(8,128)}), f32[32,8,128]{2,1,0:T(8,128)S(1)}, u32[]{:S(2)}, u32[]{:S(2)}) async-start(f32[32,8,128]{2,1,0:T(8,128)} %get-tuple-element.55), calls=%async_computation | async-start | bytes 262144 | tf_op jit(solution)/shard_map/all_to_all | solution.py:557
  51.0 2.1 %copy-start = (bf16[3,2560,256]{2,1,0:T(8,128)(2,1)S(1)}, bf16[3,2560,256]{2,1,0:T(8,128)(2,1)}, u32[]{:S(2)}) copy-start(bf16[3,2560,256]{2,1,0:T(8,128)(2,1)} %get-tuple-element.43.w_low_ref) | copy-start | bytes 11796484
  53.1 1.2 %copy-start.4 = (f32[640,384]{1,0:T(8,128)S(1)}, f32[640,384]{1,0:T(8,128)}, u32[]{:S(2)}) copy-start(f32[640,384]{1,0:T(8,128)} %get-tuple-element.44.dv_ref) | copy-start | bytes 2949124
  54.3 1.1 %copy-start.5 = (f32[512,384]{1,0:T(8,128)S(1)}, f32[512,384]{1,0:T(8,128)}, u32[]{:S(2)}) copy-start(f32[512,384]{1,0:T(8,128)} %get-tuple-element.45.dq_ref) | copy-start | bytes 2359300
  55.5 1.0 %copy-start.8 = (bf16[512,384]{1,0:T(8,128)(2,1)S(1)}, bf16[512,384]{1,0:T(8,128)(2,1)}, u32[]{:S(2)}) copy-start(bf16[512,384]{1,0:T(8,128)(2,1)} %get-tuple-element.47.dk_cross_ref) | copy-start | bytes 1179652
  59.5 17.7 %collective-permute-start.1 = (bf16[1024,384]{1,0:T(8,128)(2,1)}, bf16[1024,384]{1,0:T(8,128)(2,1)S(1)}, u32[]{:S(2)}, u32[]{:S(2)}) collective-permute-start(bf16[1024,384]{1,0:T(8,128)(2,1)} %get-tuple-element.52), channel_id=1, source_target_pairs={{4,0},{8,4},{12,8},{16,12},{20,16},{24,20},{28,24},{32,28},{36,32}... | collective-permute-start | bytes 2359304 | tf_op jit(solution)/shard_map/ppermute | solution.py:533
  67.6 21.9 %all-to-all-start.1 = ((f32[64,8,128]{2,1,0:T(8,128)}), f32[64,8,128]{2,1,0:T(8,128)S(1)}, u32[]{:S(2)}, u32[]{:S(2)}) async-start(f32[64,8,128]{2,1,0:T(8,128)} %broadcast_in_dim.10), calls=%async_computation.1 | async-start | bytes 524288 | tf_op jit(solution)/shard_map/all_to_all | solution.py:559
  77.2 0.9 %copy-start.11 = (bf16[1024,384]{1,0:T(8,128)(2,1)}, bf16[1024,384]{1,0:T(8,128)(2,1)S(1)}, u32[]{:S(2)}) copy-start(bf16[1024,384]{1,0:T(8,128)(2,1)S(1)} %collective-permute-done.1.back_key_ref.back_value_ref) | copy-start | bytes 2359300
